TPU v7x, 128 devices: a whole 4x4x4 slice. The times are simulated.
128 devices in a mesh: sp: 16 (over z, x), dp: 8 (over y, core).
Axes of the slice: x: 4, y: 4, z: 4, core: 2. Of those that a mesh axis runs over, the one named last changes fastest.
Arguments:
- residual_in: bfloat16 [8, 2048, 2048], P('dp', 'sp'), may hold values from -6 to 6
- query_proj: bfloat16 [8, 2048, 2048], P('dp', 'sp'), may hold values from -8 to 8
- key_proj: bfloat16 [8, 2048, 512], P('dp', 'sp'), may hold values from -8 to 8
- value_proj: bfloat16 [8, 2048, 512], P('dp', 'sp'), may hold values from -6 to 6
- query_gain: float32 [128], replicated, may hold values from 0.1 to 7
- key_gain: float32 [128], replicated, may hold values from 0.1 to 7
- out_weight: bfloat16 [2048, 2048], replicated, may hold values from -0.125 to 0.125
- post_gain: float32 [2048], replicated, may hold values from 0.1 to 1.9
- pre_gain: float32 [2048], replicated, may hold values from 0.1 to 1.9
- route_ids: int32 [8, 2048, 2], P('dp', 'sp'), may hold values from 0 to 127, as said below
- group_weight: float32 [8, 2048], P('dp', 'sp'), may hold values from 0.25 to 1
- first_share: float32 [8, 2048], P('dp', 'sp'), may hold values from 0.5 to 1
- gate_weight: bfloat16 [128, 2048, 512], P(('sp', 'dp')), may hold values from -0.125 to 0.125
- up_weight: bfloat16 [128, 2048, 512], P(('sp', 'dp')), may hold values from -0.125 to 0.125
- down_weight: bfloat16 [128, 512, 2048], P(('sp', 'dp')), may hold values from -0.25 to 0.25
Outputs:
- layer_out: bfloat16 [8, 2048, 2048], P('dp', 'sp')
Inputs may be any that keep to these rules, and one draw needn't show every extreme that they name: `route_ids`: each token names two different experts of one group of 32 consecutive experts. Among the 128 tokens of one device each group is chosen by exactly 32 tokens, no expert is named by more than 4 of them, and in every draw one expert of each group is named by exactly 4 tokens of every device.
All inputs are finite; a program needn't handle non-finite values.
Results may differ from a plain program's by a relative error of at most 0.009.
The roundings to bfloat16 on the way count: a program that leaves them out, or rounds other values in their place, can miss the bound.
Values may be sent and summed in bfloat16 or wider, within the bound.
A program may use at most 128 MiB of HBM per device.

v0:
```python
import jax
import jax.numpy as jnp
from jax import lax
from jax.sharding import PartitionSpec as P

HEADS = 16
KV_HEADS = 4
HEAD_DIM = 128
GRID_W = 64


EPSILON = 1e-06


def side_by_side(arrays, axis, dim, along):
    ends, at = ([], 0)
    for a in arrays[:-1]:
        at += a.shape[along]
        ends.append(at)
    both = jnp.concatenate(arrays, axis=along)
    return tuple(jnp.split(lax.all_gather(both, axis, axis=dim, tiled=True), ends, axis=along))


def rotate_heads(raw_heads, gain_vec, positions):
    floats = raw_heads.astype(jnp.float32)
    normed = (
        floats * lax.rsqrt(jnp.mean(floats * floats, axis=-1, keepdims=True) + EPSILON) * gain_vec
    )
    quarter = raw_heads.shape[-1] // 4
    inverse = 10000.0 ** (-jnp.arange(quarter, dtype=jnp.float32) / quarter)
    grid_rows = (positions // GRID_W).astype(jnp.float32)[:, None] * inverse
    grid_cols = (positions % GRID_W).astype(jnp.float32)[:, None] * inverse
    angles = jnp.concatenate([grid_rows, grid_rows, grid_cols, grid_cols], axis=-1)[:, None, :]
    pieces = normed.reshape(normed.shape[:-1] + (2, 2, quarter))
    turned = jnp.stack([-pieces[..., 1, :], pieces[..., 0, :]], axis=-2).reshape(normed.shape)
    return (normed * jnp.cos(angles) + turned * jnp.sin(angles)).astype(jnp.bfloat16)


def attend_blocks(queries, keys_all, values_all):
    count_q, kv_count, group_size, head_width = queries.shape
    block = min(512, count_q)
    blocks = count_q // block
    scale = head_width ** (-0.5)
    zero_index = jnp.zeros((), jnp.int32)

    def one_item(item):
        which = item // kv_count
        head_index = item % kv_count
        start_row = which * block
        q_block = lax.dynamic_slice(
            queries,
            (start_row, head_index, zero_index, zero_index),
            (block, 1, group_size, head_width),
        )[:, 0]
        key_block = lax.dynamic_slice(
            keys_all, (zero_index, head_index, zero_index), (keys_all.shape[0], 1, head_width)
        )[:, 0]
        value_block = lax.dynamic_slice(
            values_all, (zero_index, head_index, zero_index), (values_all.shape[0], 1, head_width)
        )[:, 0]
        scores = (
            jnp.einsum("qgd,sd->gqs", q_block, key_block, preferred_element_type=jnp.float32)
            * scale
        )
        shifted = jnp.exp(scores - jnp.max(scores, axis=-1, keepdims=True))
        weights = (shifted / jnp.sum(shifted, axis=-1, keepdims=True)).astype(jnp.bfloat16)
        return jnp.einsum(
            "gqs,sd->qgd", weights, value_block, preferred_element_type=jnp.float32
        ).astype(jnp.bfloat16)

    results = lax.map(one_item, jnp.arange(blocks * kv_count, dtype=jnp.int32))
    results = results.reshape(blocks, kv_count, block, group_size, head_width).transpose(
        0, 2, 1, 3, 4
    )
    return results.reshape(count_q, kv_count * group_size * head_width)


def rms_scale(values, gain_vec):
    floats = values.astype(jnp.float32)
    return (
        floats * lax.rsqrt(jnp.mean(floats * floats, axis=-1, keepdims=True) + EPSILON) * gain_vec
    )


def expert_ffn(arrived, gate_weight, up_weight, down_weight):
    gated = jnp.einsum("nesd,edf->nesf", arrived, gate_weight, preferred_element_type=jnp.float32)
    lifted = jnp.einsum("nesd,edf->nesf", arrived, up_weight, preferred_element_type=jnp.float32)
    hidden = (jax.nn.silu(gated) * lifted).astype(jnp.bfloat16)
    return jnp.einsum(
        "nesf,efd->nesd", hidden, down_weight, preferred_element_type=jnp.float32
    ).astype(jnp.bfloat16)


def local(
    residual_in,
    query_proj,
    key_proj,
    value_proj,
    query_gain,
    key_gain,
    out_weight,
    post_gain,
    pre_gain,
    route_ids,
    group_weight,
    first_share,
    gate_weight,
    up_weight,
    down_weight,
):
    sp_count = lax.axis_size("sp")
    dp_count = lax.axis_size("dp")
    tokens = query_proj.shape[1]
    group_size = HEADS // KV_HEADS
    key_all, value_all = side_by_side((key_proj, value_proj), "sp", 1, 0)
    length = key_all.shape[1]
    key_positions = jnp.arange(length, dtype=jnp.int32)
    query_positions = lax.axis_index("sp") * tokens + jnp.arange(tokens, dtype=jnp.int32)
    query_turned = rotate_heads(
        query_proj.reshape(tokens, HEADS, HEAD_DIM), query_gain, query_positions
    )
    key_turned = rotate_heads(key_all.reshape(length, KV_HEADS, HEAD_DIM), key_gain, key_positions)
    attended = attend_blocks(
        query_turned.reshape(tokens, KV_HEADS, group_size, HEAD_DIM),
        key_turned,
        value_all.reshape(length, KV_HEADS, HEAD_DIM),
    )
    mixed = jnp.dot(attended, out_weight, preferred_element_type=jnp.float32).astype(jnp.bfloat16)
    stream = (residual_in[0].astype(jnp.float32) + rms_scale(mixed, post_gain)).astype(jnp.bfloat16)
    normed = rms_scale(stream, pre_gain).astype(jnp.bfloat16)
    model_width = normed.shape[1]
    local_experts = gate_weight.shape[0]
    expert_count = local_experts * sp_count * dp_count
    capacity = 4 * tokens // expert_count
    chosen = route_ids.reshape(2 * tokens)
    onehot = (chosen[:, None] == jnp.arange(expert_count, dtype=jnp.int32)[None, :]).astype(
        jnp.int32
    )
    earlier = jnp.cumsum(onehot, axis=0) - onehot
    slot_rank = jnp.sum(earlier * onehot, axis=1)
    slot_index = chosen * capacity + slot_rank
    source_row = (
        jnp.full((expert_count * capacity,), tokens, jnp.int32)
        .at[slot_index]
        .set(jnp.arange(2 * tokens, dtype=jnp.int32) // 2)
    )
    padded = jnp.concatenate([normed, jnp.zeros((1, model_width), jnp.bfloat16)], axis=0)
    outgoing = padded[source_row]
    shaped = outgoing.reshape(sp_count * dp_count, local_experts, capacity, model_width)
    answered = expert_ffn(
        lax.all_to_all(shaped, ("sp", "dp"), split_axis=0, concat_axis=0, tiled=True),
        gate_weight,
        up_weight,
        down_weight,
    )
    returned = lax.all_to_all(answered, ("sp", "dp"), split_axis=0, concat_axis=0, tiled=True)
    results = (
        returned.reshape(expert_count * capacity, model_width)[slot_index]
        .astype(jnp.float32)
        .reshape(tokens, 2, model_width)
    )
    share = first_share[0]
    weight_pair = group_weight[0][:, None] * jnp.stack([share, 1.0 - share], axis=1)
    combined = jnp.sum(weight_pair[:, :, None] * results, axis=1)
    return (
        (stream.astype(jnp.float32) + combined).astype(jnp.bfloat16).reshape(1, tokens, model_width)
    )


def solution(mesh):
    placed = (
        P("dp", "sp", None),
        P("dp", "sp", None),
        P("dp", "sp", None),
        P("dp", "sp", None),
        P(),
        P(),
        P(),
        P(),
        P(),
        P("dp", "sp", None),
        P("dp", "sp"),
        P("dp", "sp"),
        P(("sp", "dp"), None, None),
        P(("sp", "dp"), None, None),
        P(("sp", "dp"), None, None),
    )
    return jax.shard_map(
        local, mesh=mesh, in_specs=placed, out_specs=P("dp", "sp", None), check_vma=False
    )
```

profile of v0, /device:TPU:1, one launch (start us, length us, event | category | flops | bytes accessed | tf_op | source)
XLA Modules:
  0.0 258.0 jit_solution(9064251186789726735)
XLA Ops:
  11.3 2.1 copy.38
  15.9 2.1 convert_multiply_fusion.2
  22.0 4.6 %fusion.72 = (f32[2048,128]{0,1:T(8,128)}, f32[2048,128]{0,1:T(8,128)}) fusion(f32[2048,32]{0,1:T(8,128)S(1)} %get-tuple-element.123, f32[2048,32]{0,1:T(8,128)S(1)} %get-tuple-element.122), kind=kLoop, calls=%fused_computation.69 | loop fusion | flops 786432 | bytes 2621440 | tf_op jit(solution)/shard_map/cos | solution.py:36
  27.7 40.7 %all-gather.2.cloned.1.call-done = bf16[2,2048,512]{1,2,0:T(8,128)(2,1)} async-done(((bf16[2,128,512]{1,2,0:T(8,128)(2,1)}), bf16[2,2048,512]{1,2,0:T(8,128)(2,1)}) %all-gather.2.cloned.1.call-update) | async-done | bytes 4194320 | tf_op jit(solution)/shard_map/all_gather | solution.py:21
  68.5 4.3 %slice_convert_fusion = (f32[1,2048,512]{1,2,0:T(8,128)S(1)}, bf16[1,2048,512]{1,2,0:T(8,128)(2,1)}) fusion(bf16[2,2048,512]{1,2,0:T(8,128)(2,1)} %all-gather.2.cloned.1.call-done), kind=kLoop, calls=%fused_computation.38 | loop fusion | flops 1048576 | bytes 10485760 | tf_op jit(solution)/shard_map/convert_element_type | solution.py:25
  76.1 2.8 %fusion.29 = bf16[2048,4,128]{0,2,1:T(8,128)(2,1)} fusion(f32[2048,4,2,2,32]{0,4,3,2,1:T(8,128)S(1)} %pad_maximum_fusion, f32[2048,4,128]{0,2,1:T(8,128)S(1)} %bitcast.174, f32[2048,128]{0,1:T(8,128)S(1)} %copy-done.3, f32[2048,128]{0,1:T(8,128)S(1)} %copy-done.2, f32[128]{0:T(128)S(1)} %copy-done.11, f32[2048,4]{0,1:T(4,128)S(1)} %add_rsqrt_fusion), kind=kLoop, calls=%fused_computation.30 | loop fusion | flops 6291456 | bytes 12616192 | tf_op jit(solution)/shard_map/convert_element_type | solution.py:36
  78.9 49.5 %while.12 = (s32[]{:T(128)}, bf16[4,128,4,128]{1,3,2,0:T(8,128)(2,1)S(1)}, s32[4]{0:T(128)S(1)}, bf16[2048,4,128]{0,2,1:T(8,128)(2,1)}, bf16[2048,4,128]{0,2,1:T...) while((s32[]{:T(128)}, ...), condition=%wide.region_5.6_spmd, body=%wide.region_2.5_spmd.sunk | while | flops 546378240 | bytes 34871072 | solution.py:71
  81.4 1.8 fusion.115
  83.2 1.9 copy-done.1
  86.3 5.0 %fusion.117 = bf16[4,128,4,128]{1,3,2,0:T(8,128)(2,1)S(1)} fusion(bf16[4,128,4,128]{1,3,2,0:T(8,128)(2,1)S(1)} %get-tuple-element.178, s32[]{:T(128)} %get-tuple-element.177, f32[4,128]{1,0:T(4,128)S(1)} %fusion.116, bf16[2048,4,128]{0,2,1:T(8,128)(2,1)} %get-tuple-element.190, s32[]{:T(128)S(6)} %select_n.109, f32[2048,128,4]{1,0,2:T(8,128)} %copy-done.1), kind=kOutput, calls=%fused_computation.14.clone.1 | convolution fusion | flops 273746432 | bytes 9046532 | tf_op jit(solution)/shard_map/while/body/eval_jaxpr/gqs,sd->qgd/dot_general | solution.py:67
  93.8 1.8 fusion.115
  95.6 1.9 copy-done.1
  98.7 5.0 %fusion.117 = bf16[4,128,4,128]{1,3,2,0:T(8,128)(2,1)S(1)} fusion(bf16[4,128,4,128]{1,3,2,0:T(8,128)(2,1)S(1)} %get-tuple-element.178, s32[]{:T(128)} %get-tuple-element.177, f32[4,128]{1,0:T(4,128)S(1)} %fusion.116, bf16[2048,4,128]{0,2,1:T(8,128)(2,1)} %get-tuple-element.190, s32[]{:T(128)S(6)} %select_n.109, f32[2048,128,4]{1,0,2:T(8,128)} %copy-done.1), kind=kOutput, calls=%fused_computation.14.clone.1 | convolution fusion | flops 273746432 | bytes 9046532 | tf_op jit(solution)/shard_map/while/body/eval_jaxpr/gqs,sd->qgd/dot_general | solution.py:67
  106.2 1.8 fusion.115
  108.0 1.9 copy-done.1
  111.1 5.0 %fusion.117 = bf16[4,128,4,128]{1,3,2,0:T(8,128)(2,1)S(1)} fusion(bf16[4,128,4,128]{1,3,2,0:T(8,128)(2,1)S(1)} %get-tuple-element.178, s32[]{:T(128)} %get-tuple-element.177, f32[4,128]{1,0:T(4,128)S(1)} %fusion.116, bf16[2048,4,128]{0,2,1:T(8,128)(2,1)} %get-tuple-element.190, s32[]{:T(128)S(6)} %select_n.109, f32[2048,128,4]{1,0,2:T(8,128)} %copy-done.1), kind=kOutput, calls=%fused_computation.14.clone.1 | convolution fusion | flops 273746432 | bytes 9046532 | tf_op jit(solution)/shard_map/while/body/eval_jaxpr/gqs,sd->qgd/dot_general | solution.py:67
  118.6 1.8 fusion.115
  120.4 1.9 copy-done.1
  123.4 5.0 %fusion.117 = bf16[4,128,4,128]{1,3,2,0:T(8,128)(2,1)S(1)} fusion(bf16[4,128,4,128]{1,3,2,0:T(8,128)(2,1)S(1)} %get-tuple-element.178, s32[]{:T(128)} %get-tuple-element.177, f32[4,128]{1,0:T(4,128)S(1)} %fusion.116, bf16[2048,4,128]{0,2,1:T(8,128)(2,1)} %get-tuple-element.190, s32[]{:T(128)S(6)} %select_n.109, f32[2048,128,4]{1,0,2:T(8,128)} %copy-done.1), kind=kOutput, calls=%fused_computation.14.clone.1 | convolution fusion | flops 273746432 | bytes 9046532 | tf_op jit(solution)/shard_map/while/body/eval_jaxpr/gqs,sd->qgd/dot_general | solution.py:67
  128.5 4.8 %multiply_reduce_fusion.2 = (f32[128]{0:T(128)S(1)}, f32[128,2048]{1,0:T(8,128)S(1)}) fusion(bf16[128,2048]{0,1:T(8,128)(2,1)S(1)} %bitcast.181, bf16[2048,2048]{1,0:T(8,128)(2,1)} %param.23), kind=kOutput, calls=%fused_computation.65 | convolution fusion | flops 1074790272 | bytes 9961984 | tf_op jit(solution)/shard_map/dot_general | solution.py:128
  133.9 3.3 %gather_fusion = bf16[512,2048]{1,0:T(8,128)(2,1)} fusion(bf16[129,2048]{1,0:T(8,128)(2,1)S(1)} %concatenate.35, s32[1024]{0:T(1024)S(1)} %pad_clamp_fusion.1), kind=kCustom, calls=%fused_computation | custom fusion | bytes 4196352 | tf_op jit(solution)/shard_map/gather | solution.py:148
  137.3 4.1 %reshape.477 = bf16[128,1,4,2048]{3,2,0,1:T(4,128)(2,1)} reshape(bf16[512,2048]{1,0:T(8,128)(2,1)} %gather_fusion) | data formatting | bytes 4194304 | tf_op jit(solution)/shard_map/reshape | solution.py:149
  141.4 39.0 %all_to_all.10 = bf16[128,1,4,2048]{3,2,1,0:T(4,128)(2,1)S(1)} all-to-all(bf16[128,1,4,2048]{3,2,1,0:T(4,128)(2,1)} %bitcast.177), channel_id=1, replica_groups=mesh['sp'=16,'dp'=8] {'sp','dp'}, dimensions={0} | all-to-all | bytes 4194304 | tf_op jit(solution)/shard_map/all_to_all | solution.py:151
  181.7 3.4 %fusion.41 = f32[128,1,4,512]{3,0,2,1:T(8,128)} fusion(bf16[1,2048,512]{2,1,0:T(8,128)(2,1)S(1)} %copy-done.14, bf16[128,1,4,2048]{3,2,1,0:T(4,128)(2,1)S(1)} %all_to_all.10), kind=kOutput, calls=%fused_computation.52 | convolution fusion | flops 1073741824 | bytes 5242880 | tf_op jit(solution)/shard_map/nesd,edf->nesf/dot_general | solution.py:86
  185.1 7.5 %fusion.30 = bf16[128,1,4,2048]{3,0,2,1:T(8,128)(2,1)} fusion(bf16[1,512,2048]{2,1,0:T(8,128)(2,1)S(1)} %copy-done, bf16[1,2048,512]{2,1,0:T(8,128)(2,1)} %param.30, bf16[128,1,4,2048]{3,2,1,0:T(4,128)(2,1)} %copy-done.4, f32[128,1,4,512]{3,0,2,1:T(8,128)} %fusion.41), kind=kOutput, calls=%fused_computation.34 | convolution fusion | flops 2150105088 | bytes 9437184 | tf_op jit(solution)/shard_map/nesf,efd->nesd/dot_general | solution.py:89
  192.6 4.5 %copy.49 = bf16[128,1,4,2048]{3,2,1,0:T(4,128)(2,1)} copy(bf16[128,1,4,2048]{3,0,2,1:T(8,128)(2,1)} %fusion.30) | data formatting | bytes 4194304 | tf_op jit(solution)/shard_map/convert_element_type | solution.py:91
  197.2 5.8 %all-to-all-start.1 = ((bf16[128,1,4,2048]{3,2,1,0:T(4,128)(2,1)}), bf16[128,1,4,2048]{3,2,1,0:T(4,128)(2,1)}, u32[]{:S(2)}, u32[]{:S(2)}) async-start(bf16[128,1,4,2048]{3,2,1,0:T(4,128)(2,1)} %copy.49), calls=%async_computation.1 | async-start | bytes 4194304 | tf_op jit(solution)/shard_map/all_to_all | solution.py:156
  203.2 29.7 %all-to-all-done.1 = bf16[128,1,4,2048]{3,2,1,0:T(4,128)(2,1)} async-done(((bf16[128,1,4,2048]{3,2,1,0:T(4,128)(2,1)}), bf16[128,1,4,2048]{3,2,1,0:T(4,128)(2,1)}, u32[]{:S(2)}, u32[]{:S(2)}) %all-to-all-start.1) | async-done | bytes 2097184 | tf_op jit(solution)/shard_map/all_to_all | solution.py:156
  232.9 4.0 %reshape.483 = bf16[512,2048]{1,0:T(8,128)(2,1)} reshape(bf16[128,1,4,2048]{3,2,1,0:T(4,128)(2,1)} %all-to-all-done.1) | data formatting | bytes 4194304 | tf_op jit(solution)/shard_map/reshape | solution.py:158
  236.8 5.2 %gather_fusion.1 = bf16[256,2048]{1,0:T(8,128)(2,1)} fusion(bf16[512,2048]{1,0:T(8,128)(2,1)} %reshape.483, s32[1024]{0:T(1024)S(1)} %pad_clamp_fusion), kind=kCustom, calls=%fused_computation.1 | custom fusion | bytes 2098176 | tf_op jit(solution)/shard_map/gather | solution.py:158
  242.0 3.4 %reshape.490 = f32[128,2,2048]{2,1,0:T(2,128)} reshape(bf16[256,2048]{1,0:T(8,128)(2,1)} %gather_fusion.1) | data formatting | bytes 3145728 | tf_op jit(solution)/shard_map/convert_element_type | solution.py:159
  245.4 4.8 %multiply_reduce_fusion.1 = f32[128,2048]{1,0:T(8,128)S(1)} fusion(f32[128,2,2048]{2,1,0:T(2,128)} %reshape.490, f32[128,2]{1,0:T(8,128)S(1)} %copy.41), kind=kLoop, calls=%fused_computation.46 | loop fusion | flops 786432 | bytes 3146752 | tf_op jit(solution)/shard_map/reduce_sum | solution.py:164
  (97 shorter events, 25.4 us)
Async XLA Ops:
  6.5 178.6 %copy-start = (bf16[1,512,2048]{2,1,0:T(8,128)(2,1)S(1)}, bf16[1,512,2048]{2,1,0:T(8,128)(2,1)}, u32[]{:S(2)}) copy-start(bf16[1,512,2048]{2,1,0:T(8,128)(2,1)} %param.31) | copy-start | bytes 6291460
  6.5 9.1 %copy-start.9 = (s32[1,128,2]{1,2,0:T(2,128)S(1)}, s32[1,128,2]{1,2,0:T(2,128)}, u32[]{:S(2)}) copy-start(s32[1,128,2]{1,2,0:T(2,128)} %param.26) | copy-start | bytes 3076
  6.5 61.9 %all-gather.2.cloned.1.call-start = ((), (), s32[]{:S(2)}) async-start(), calls=%async_computation.2 | async-start | bytes 4456448 | tf_op jit(solution)/shard_map/all_gather | solution.py:21
  21.7 4.9 %copy-start.10 = (f32[128]{0:T(128)S(1)}, f32[128]{0:T(128)}, u32[]{:S(2)}) copy-start(f32[128]{0:T(128)} %param.21) | copy-start | bytes 1540
  74.5 1.2 copy-start.2
  74.5 1.5 copy-start.3
  74.5 1.5 copy-start.11
  76.1 2.8 %copy-start.5 = (bf16[4,128,4,128]{1,3,2,0:T(8,128)(2,1)S(1)}, bf16[4,128,4,128]{1,3,2,0:T(8,128)(2,1)}, u32[]{:S(2)}) copy-start(bf16[4,128,4,128]{1,3,2,0:T(8,128)(2,1)} %custom-call.4) | copy-start | bytes 1572868
  83.2 1.9 copy-start.1
  95.6 1.9 copy-start.1
  108.0 1.9 copy-start.1
  120.4 1.9 copy-start.1
  128.4 4.8 %copy-start.6 = (bf16[1,128,2048]{2,1,0:T(8,128)(2,1)S(1)}, bf16[1,128,2048]{2,1,0:T(8,128)(2,1)}, u32[]{:S(2)}) copy-start(bf16[1,128,2048]{2,1,0:T(8,128)(2,1)} %param.17) | copy-start | bytes 1572868
  128.4 4.8 %copy-start.7 = (f32[2048]{0:T(1024)S(1)}, f32[2048]{0:T(1024)}, u32[]{:S(2)}) copy-start(f32[2048]{0:T(1024)} %param.24) | copy-start | bytes 24580
  128.4 5.2 %copy-start.8 = (f32[2048]{0:T(1024)S(1)}, f32[2048]{0:T(1024)}, u32[]{:S(2)}) copy-start(f32[2048]{0:T(1024)} %param.25) | copy-start | bytes 24580
  141.4 40.3 %copy-start.14 = (bf16[1,2048,512]{2,1,0:T(8,128)(2,1)S(1)}, bf16[1,2048,512]{2,1,0:T(8,128)(2,1)}, u32[]{:S(2)}) copy-start(bf16[1,2048,512]{2,1,0:T(8,128)(2,1)} %param.29) | copy-start | bytes 6291460
  180.4 1.3 copy-start.4
  192.6 10.4 %copy-start.12 = (f32[1,128]{1,0:T(1,128)S(1)}, f32[1,128]{1,0:T(1,128)}, u32[]{:S(2)}) copy-start(f32[1,128]{1,0:T(1,128)} %param.28) | copy-start | bytes 1540
  192.6 10.4 %copy-start.13 = (f32[1,128]{1,0:T(1,128)S(1)}, f32[1,128]{1,0:T(1,128)}, u32[]{:S(2)}) copy-start(f32[1,128]{1,0:T(1,128)} %param.27) | copy-start | bytes 1540
  197.2 35.7 %all-to-all-start.1 = ((bf16[128,1,4,2048]{3,2,1,0:T(4,128)(2,1)}), bf16[128,1,4,2048]{3,2,1,0:T(4,128)(2,1)}, u32[]{:S(2)}, u32[]{:S(2)}) async-start(bf16[128,1,4,2048]{3,2,1,0:T(4,128)(2,1)} %copy.49), calls=%async_computation.1 | async-start | bytes 4194304 | tf_op jit(solution)/shard_map/all_to_all | solution.py:156
Sparse Core Ops, SparseCore 0:
  9.6 58.7 all-gather.1
where the time goes:
time: 259 us; the launch traced here: 258 us
  waiting for transfers between devices  70.4 us (27%)
  local copies, waits for them, and re-layouts  46.1 us (18%)
  matrix products  42.7 us (16%)
  blocking collectives  39 us (15%)
  other arithmetic  32.2 us (12%)
  between operations  13.8 us (5%)
  loops' own time  7.97 us (3%)
  starting transfers between devices  5.81 us (2%)
    all_gather x1, waiting for transfers between devices, side_by_side(): lax.all_gather(both, axis, axis=dim, tiled=True)  40.7 us
    all_to_all x1, blocking collectives, local(): lax.all_to_all(shaped, ('sp', 'dp'), split_axis=0, concat_axis=0, tiled=T...  39 us
    all_to_all x1, waiting for transfers between devices, local(): lax.all_to_all(answered, ('sp', 'dp'), split_axis=0, concat_axis=0, tiled...  29.7 us
    dot_general x4, matrix products, one_item(): jnp.einsum('gqs,sd->qgd', weights, value_block, preferred_element_type=jn...  19.8 us
    another operation x1, loops' own time, attend_blocks(): results = lax.map(one_item, jnp.arange(blocks * kv_count, dtype=jnp.int32))  7.97 us
    while x8, local copies, waits for them, and re-layouts  7.68 us
    unnamed x33, local copies, waits for them, and re-layouts  7.64 us
    dot_general x1, matrix products, expert_ffn(): jnp.einsum('nesf,efd->nesd', hidden, down_weight, preferred_element_type=...  7.52 us
  transfers between devices with their start and end apart: 2, of which 2 were waited for; matrix products, arithmetic and copies ran while one was open for 7% of the time, Pallas kernels for 0%

commit v1 on v0

v1 whole, which is shorter than its diff:
```python
import functools

import jax
import jax.numpy as jnp
import numpy as np
from jax import lax
from jax.experimental import pallas as pl
from jax.experimental.pallas import tpu as pltpu
from jax.sharding import PartitionSpec as P

HEADS = 16
KV_HEADS = 4
HEAD_DIM = 128
GRID_W = 64
RING = 4
EPSILON = 1e-06
MESH = pl.DeviceIdType.MESH
F32 = jnp.float32
BF16 = jnp.bfloat16


def angle_tables():
    quarter = HEAD_DIM // 4
    inverse = (np.float32(10000.0) ** (-np.arange(quarter, dtype=np.float32) / quarter)).astype(
        np.float32
    )
    places = np.concatenate([np.arange(32), np.arange(GRID_W)]).astype(np.float32)
    angles = places[:, None] * np.tile(inverse, 4)[None, :]
    return np.stack([np.cos(angles), np.sin(angles)]).astype(np.float32)


def position():
    s = lax.axis_index("sp")
    d = lax.axis_index("dp")
    return s // RING, s % RING, d // 2, d % 2


def at(z, x, y, c):
    return (
        ((z + 2 * RING) % RING) * RING + (x + 2 * RING) % RING,
        ((y + 2 * RING) % RING) * 2 + c,
    )


def turn(heads, gain, cos, sin):
    normed = (
        heads * lax.rsqrt(jnp.mean(heads * heads, axis=-1, keepdims=True) + EPSILON) * gain
    )
    lane = lax.broadcasted_iota(jnp.int32, normed.shape, 1)
    turned = jnp.where(
        (lane // 32) % 2 == 0, -pltpu.roll(normed, 96, 1), pltpu.roll(normed, 32, 1)
    )
    return (normed * cos + turned * sin).astype(BF16)


def attention_kernel(
    q_hbm, k_hbm, v_hbm, w_hbm, res_hbm, table_ref, qg_ref, kg_ref, postg_ref, preg_ref,
    stream_ref, normed_ref,
    kv, qt, q_raw, k_raw, v_raw, w, res, top, total, acc, att, mixed,
    local_sem, send_sem, recv_sem,
):
    z, x, y, c = position()
    right, left = at(z, x + 1, y, c), at(z, x - 1, y, c)
    up, down = at(z + 1, x, y, c), at(z - 1, x, y, c)

    loads = []
    for i, (src, dst) in enumerate(
        [(k_hbm, k_raw), (v_hbm, v_raw), (q_hbm, q_raw), (res_hbm, res), (w_hbm, w)]
    ):
        load = pltpu.make_async_copy(src, dst, local_sem.at[i])
        load.start()
        loads.append(load)

    barrier = pltpu.get_barrier_semaphore()
    for peer in (right, left, up, down):
        pl.semaphore_signal(barrier, inc=1, device_id=peer, device_id_type=MESH)

    lane = lax.broadcasted_iota(jnp.int32, (GRID_W, HEAD_DIM), 1)

    def table(which):
        halves = []
        for part in range(2):
            row = table_ref[which, pl.ds(2 * (z * RING + x) + part, 1), :]
            halves.append(jnp.where(lane < 64, row, table_ref[which, 32 : 32 + GRID_W, :]))
        return jnp.concatenate(halves, axis=0)

    cos, sin = table(0), table(1)
    loads[0].wait()
    for h in range(KV_HEADS):
        raw = k_raw[:, h * 128 : (h + 1) * 128].astype(F32)
        kv[h // 2, 0, 0, :, (h % 2) * 128 : (h % 2 + 1) * 128] = turn(raw, kg_ref[...], cos, sin)
    loads[1].wait()
    for half in range(2):
        kv[half, 0, 0, :, 256:512] = v_raw[:, half * 256 : (half + 1) * 256]
    pl.semaphore_wait(barrier, 4)

    messages = {}
    first = {0: (right, left), 1: (up, down)}
    second = {0: (up, down), 1: (right, left)}

    def message(name, src, dst, peer):
        i = len(messages)
        messages[name] = pltpu.make_async_remote_copy(
            src_ref=src,
            dst_ref=dst,
            send_sem=send_sem.at[i],
            recv_sem=recv_sem.at[i],
            device_id=peer,
            device_id_type=MESH,
        )

    low, high = pl.ds(0, 64), pl.ds(64, 64)
    for p in range(2):
        plus, minus = first[p]
        message(("own+", p), kv.at[p, 0, 0], kv.at[p, 0, 3], plus)
        message(("own-", p), kv.at[p, 0, 0], kv.at[p, 0, 1], minus)
        message(("relay+", p), kv.at[p, 0, 3, low], kv.at[p, 0, 2, low], plus)
        message(("relay-", p), kv.at[p, 0, 1, high], kv.at[p, 0, 2, high], minus)
        plus, minus = second[p]
        for r in range(4):
            message(("far+", p, r), kv.at[p, 0, r], kv.at[p, 3, r], plus)
            message(("far-", p, r), kv.at[p, 0, r], kv.at[p, 1, r], minus)
            message(("last+", p, r), kv.at[p, 3, r, low], kv.at[p, 2, r, low], plus)
            message(("last-", p, r), kv.at[p, 1, r, high], kv.at[p, 2, r, high], minus)

    def start(kind, *key):
        for sign in "+-":
            messages[(kind + sign,) + key].start()

    def arrived(kind, *key):
        for sign in "+-":
            messages[(kind + sign,) + key].wait_recv()

    start("own", 0)
    start("own", 1)
    start("far", 0, 0)
    start("far", 1, 0)

    loads[2].wait()
    for h in range(HEADS):
        raw = q_raw[:, h * 128 : (h + 1) * 128].astype(F32)
        qt[h // 4, (h % 4) * 128 : (h % 4 + 1) * 128, :] = turn(raw, qg_ref[...], cos, sin)

    for p in range(2):
        arrived("own", p)
        start("relay", p)
        start("far", p, 3)
        start("far", p, 1)
    for p in range(2):
        arrived("far", p, 0)
        start("last", p, 0)
    for p in range(2):
        arrived("relay", p)
        start("far", p, 2)

    scale = float(np.log2(np.e) / np.sqrt(HEAD_DIM))

    def attend(r, opening):
        def one(g, carry):
            p, h = g // 2, g % 2
            keys = kv[p, r, :, :, pl.ds(pl.multiple_of(h * 128, 128), 128)].reshape(512, 128)
            values = kv[p, r, :, :, pl.ds(pl.multiple_of(256 + h * 128, 128), 128)].reshape(
                512, 128
            )
            scores = lax.dot_general(
                qt[g], keys, (((1,), (1,)), ((), ())), preferred_element_type=F32
            )
            peak = jnp.max(scores, axis=-1, keepdims=True)
            if not opening:
                before = top[g]
                peak = jnp.maximum(peak, before)
            weights = jnp.exp2((scores - peak) * scale)
            summed = jnp.sum(weights, axis=-1, keepdims=True)
            out = jnp.dot(weights.astype(BF16), values, preferred_element_type=F32)
            if not opening:
                shrink = jnp.exp2((before - peak) * scale)
                summed += total[g] * shrink
                out += acc[g] * shrink
            top[g] = peak
            total[g] = summed
            acc[g] = out
            return carry

        lax.fori_loop(0, KV_HEADS, one, 0)

    attend(0, True)
    for r in (3, 1):
        for p in range(2):
            arrived("far", p, r)
            start("last", p, r)
    for p in range(2):
        arrived("far", p, 2)
        start("last", p, 2)
    attend(3, False)
    attend(1, False)
    for p in range(2):
        for r in range(4):
            arrived("last", p, r)
    attend(2, False)

    for h in range(HEADS):
        rows = slice((h % 4) * 128, (h % 4 + 1) * 128)
        att[:, h * 128 : (h + 1) * 128] = (acc[h // 4, rows, :] / total[h // 4, rows, :]).astype(
            BF16
        )
    loads[3].wait()
    loads[4].wait()

    def project(n, carry):
        cols = pl.ds(pl.multiple_of(n * 512, 512), 512)
        mixed[:, cols] = jnp.dot(att[...], w[:, cols], preferred_element_type=F32).astype(BF16)
        return carry

    lax.fori_loop(0, 4, project, 0)

    def norm(n, carry):
        rows = pl.ds(pl.multiple_of(n * 16, 16), 16)
        m = mixed[rows, :].astype(F32)
        m = m * lax.rsqrt(jnp.mean(m * m, axis=-1, keepdims=True) + EPSILON) * postg_ref[...]
        stream = (res[rows, :].astype(F32) + m).astype(BF16)
        stream_ref[rows, :] = stream
        s = stream.astype(F32)
        s = s * lax.rsqrt(jnp.mean(s * s, axis=-1, keepdims=True) + EPSILON) * preg_ref[...]
        normed_ref[rows, :] = s.astype(BF16)
        return carry

    lax.fori_loop(0, 8, norm, 0)
    for m in messages.values():
        m.wait_send()


def attention(q, k, v, w, res, query_gain, key_gain, post_gain, pre_gain):
    hbm = pl.BlockSpec(memory_space=pl.ANY)
    vmem = pl.BlockSpec(memory_space=pltpu.VMEM)
    tokens, width = q.shape
    return pl.pallas_call(
        attention_kernel,
        out_shape=[jax.ShapeDtypeStruct((tokens, width), BF16)] * 2,
        in_specs=[hbm] * 5 + [vmem] * 5,
        out_specs=[vmem] * 2,
        scratch_shapes=[
            pltpu.VMEM((2, 4, 4, 128, 512), BF16),
            pltpu.VMEM((4, 512, 128), BF16),
            pltpu.VMEM((tokens, width), BF16),
            pltpu.VMEM((tokens, 512), BF16),
            pltpu.VMEM((tokens, 512), BF16),
            pltpu.VMEM((width, width), BF16),
            pltpu.VMEM((tokens, width), BF16),
            pltpu.VMEM((4, 512, 1), F32),
            pltpu.VMEM((4, 512, 1), F32),
            pltpu.VMEM((4, 512, 128), F32),
            pltpu.VMEM((tokens, width), BF16),
            pltpu.VMEM((tokens, width), BF16),
            pltpu.SemaphoreType.DMA((5,)),
            pltpu.SemaphoreType.DMA((40,)),
            pltpu.SemaphoreType.DMA((40,)),
        ],
        compiler_params=pltpu.CompilerParams(
            collective_id=0, has_side_effects=True, vmem_limit_bytes=60 * 1024 * 1024
        ),
        name="attention",
    )(
        q, k, v, w, res, jnp.asarray(angle_tables()), query_gain.reshape(1, -1),
        key_gain.reshape(1, -1), post_gain.reshape(1, -1), pre_gain.reshape(1, -1),
    )


def expert_ffn(arrived, gate_weight, up_weight, down_weight):
    gated = jnp.einsum("nesd,edf->nesf", arrived, gate_weight, preferred_element_type=jnp.float32)
    lifted = jnp.einsum("nesd,edf->nesf", arrived, up_weight, preferred_element_type=jnp.float32)
    hidden = (jax.nn.silu(gated) * lifted).astype(jnp.bfloat16)
    return jnp.einsum(
        "nesf,efd->nesd", hidden, down_weight, preferred_element_type=jnp.float32
    ).astype(jnp.bfloat16)


def local(
    residual_in,
    query_proj,
    key_proj,
    value_proj,
    query_gain,
    key_gain,
    out_weight,
    post_gain,
    pre_gain,
    route_ids,
    group_weight,
    first_share,
    gate_weight,
    up_weight,
    down_weight,
):
    sp_count = lax.axis_size("sp")
    dp_count = lax.axis_size("dp")
    tokens = query_proj.shape[1]
    stream, normed = attention(
        query_proj[0], key_proj[0], value_proj[0], out_weight, residual_in[0],
        query_gain, key_gain, post_gain, pre_gain,
    )
    model_width = normed.shape[1]
    local_experts = gate_weight.shape[0]
    expert_count = local_experts * sp_count * dp_count
    capacity = 4 * tokens // expert_count
    chosen = route_ids.reshape(2 * tokens)
    onehot = (chosen[:, None] == jnp.arange(expert_count, dtype=jnp.int32)[None, :]).astype(
        jnp.int32
    )
    earlier = jnp.cumsum(onehot, axis=0) - onehot
    slot_rank = jnp.sum(earlier * onehot, axis=1)
    slot_index = chosen * capacity + slot_rank
    source_row = (
        jnp.full((expert_count * capacity,), tokens, jnp.int32)
        .at[slot_index]
        .set(jnp.arange(2 * tokens, dtype=jnp.int32) // 2)
    )
    padded = jnp.concatenate([normed, jnp.zeros((1, model_width), jnp.bfloat16)], axis=0)
    outgoing = padded[source_row]
    shaped = outgoing.reshape(sp_count * dp_count, local_experts, capacity, model_width)
    answered = expert_ffn(
        lax.all_to_all(shaped, ("sp", "dp"), split_axis=0, concat_axis=0, tiled=True),
        gate_weight,
        up_weight,
        down_weight,
    )
    returned = lax.all_to_all(answered, ("sp", "dp"), split_axis=0, concat_axis=0, tiled=True)
    results = (
        returned.reshape(expert_count * capacity, model_width)[slot_index]
        .astype(jnp.float32)
        .reshape(tokens, 2, model_width)
    )
    share = first_share[0]
    weight_pair = group_weight[0][:, None] * jnp.stack([share, 1.0 - share], axis=1)
    combined = jnp.sum(weight_pair[:, :, None] * results, axis=1)
    return (
        (stream.astype(jnp.float32) + combined).astype(jnp.bfloat16).reshape(1, tokens, model_width)
    )


def solution(mesh):
    placed = (
        P("dp", "sp", None),
        P("dp", "sp", None),
        P("dp", "sp", None),
        P("dp", "sp", None),
        P(),
        P(),
        P(),
        P(),
        P(),
        P("dp", "sp", None),
        P("dp", "sp"),
        P("dp", "sp"),
        P(("sp", "dp"), None, None),
        P(("sp", "dp"), None, None),
        P(("sp", "dp"), None, None),
    )
    return jax.shard_map(
        local, mesh=mesh, in_specs=placed, out_specs=P("dp", "sp", None), check_vma=False
    )
```

time: 259 us -> 174 us (0.67)
  Pallas kernels: 0 us -> 51.2 us
  waiting for transfers between devices: 70.4 us -> 29.7 us
  matrix products: 42.7 us -> 10.9 us
  other arithmetic: 32.2 us -> 6.92 us
  local copies, waits for them, and re-layouts: 46.1 us -> 28 us
  between operations: 13.8 us -> 0.16 us
  loops' own time: 7.97 us -> 0 us
    pallas_call x0 -> x1, Pallas kernels: none -> 51.2 us  [attention(): pl.pallas_call(attention_kernel, out_shape=[jax.ShapeDtypeStruct((tokens,...]
    all_gather x1 -> x0, waiting for transfers between devices: 40.7 us -> none  [side_by_side(): lax.all_gather(both, axis, axis=dim, tiled=True)]
    dot_general x9 -> x0, matrix products: 31.8 us -> none  [the longest x4 19.8 us: one_item(): jnp.einsum('gqs,sd->qgd', weights, value_block, preferred_element_type=jn...]
    convert_element_type x7 -> x0, other arithmetic: 9.6 us -> none  [the longest x2 5.45 us: rotate_heads(): floats = raw_heads.astype(jnp.float32)]
    another operation x1 -> x0, loops' own time: 7.97 us -> none  [attend_blocks(): results = lax.map(one_item, jnp.arange(blocks * kv_count, dtype=jnp.int32))]
    while x8 -> x0, local copies, waits for them, and re-layouts: 7.68 us -> none
    unnamed x33 -> x14, local copies, waits for them, and re-layouts: 7.64 us -> 2.25 us
    cos x2 -> x0, other arithmetic: 4.7 us -> none  [rotate_heads(): jnp.cos(angles)]
  transfers between devices with their start and end apart: 2 -> 1, of which waited for: 2 -> 1; matrix products, arithmetic and copies ran while one was open for 7% -> 0% of each run, Pallas kernels for 0% -> 0%
where the time goes in v1:
time: 174 us
  Pallas kernels  51.2 us (29%)
  blocking collectives  40.8 us (23%)
  waiting for transfers between devices  29.7 us (17%)
  local copies, waits for them, and re-layouts  28 us (16%)
  matrix products  10.9 us (6%)
  other arithmetic  6.92 us (4%)
  starting transfers between devices  5.94 us (3%)
    pallas_call x1, Pallas kernels, attention(): pl.pallas_call(attention_kernel, out_shape=[jax.ShapeDtypeStruct((tokens,...  51.2 us
    all_to_all x1, blocking collectives, local(): lax.all_to_all(shaped, ('sp', 'dp'), split_axis=0, concat_axis=0, tiled=T...  40.8 us
    all_to_all x1, waiting for transfers between devices, local(): lax.all_to_all(answered, ('sp', 'dp'), split_axis=0, concat_axis=0, tiled...  29.7 us
    dot_general x1, matrix products, expert_ffn(): jnp.einsum('nesf,efd->nesd', hidden, down_weight, preferred_element_type=...  7.52 us
    all_to_all x1, starting transfers between devices, local(): lax.all_to_all(answered, ('sp', 'dp'), split_axis=0, concat_axis=0, tiled...  5.94 us
    reduce_sum x1, other arithmetic, local(): combined = jnp.sum(weight_pair[:, :, None] * results, axis=1)  4.86 us
    convert_element_type x1, local copies, waits for them, and re-layouts, expert_ffn(): return jnp.einsum('nesf,efd->nesd', hidden, down_weight, preferred_elemen...  4.5 us
    gather x1, local copies, waits for them, and re-layouts, local(): returned.reshape(expert_count * capacity, model_width)[slot_index]  4.22 us
  transfers between devices with their start and end apart: 1, of which 1 were waited for; matrix products, arithmetic and copies ran while one was open for 0% of the time, Pallas kernels for 0%

profile of v1, /device:TPU:1, one launch (start us, length us, event | category | flops | bytes accessed | tf_op | source)
XLA Modules:
  0.0 173.7 jit_solution(1777927483929742574)
XLA Ops:
  0.0 0.0 copy-start
  0.0 0.9 copy.28
  0.9 0.1 eq.29
  1.1 0.1 eq.25
  1.2 0.7 broadcast_multiply_fusion
  1.9 0.1 copy.30
  2.0 0.2 fusion.41
  2.3 0.1 copy.27
  2.4 0.1 mul.54
  2.6 0.2 fusion.43
  2.8 1.4 scatter_custom_fusion
  4.2 51.2 %attention.1 = (bf16[128,2048]{1,0:T(8,128)(2,1)}, bf16[128,2048]{1,0:T(8,128)(2,1)}) custom-call(bf16[128,2048]{1,0:T(8,128)(2,1)} %bitcast.102, bf16[128,512]{1,0:T(8,128)(2,1)} %bitcast.105, bf16[128,512]{1,0:T(8,128)(2,1)} %bitcast.106, bf16[2048,2048]{1,0:T(8,128)(2,1)} %w_hbm.1, bf16[128,2048]{1,0:T(8,128)(2,1)} %bitcast.103, ...), custom_call_target="tpu_custom_call" | custom-call | tf_op jit(solution)/shard_map/attention/pallas_call | solution.py:236
  55.4 1.1 concatenate.7
  56.5 3.3 %gather_fusion = bf16[512,2048]{1,0:T(8,128)(2,1)} fusion(bf16[129,2048]{1,0:T(8,128)(2,1)S(1)} %concatenate.7, s32[1024]{0:T(1024)S(1)} %pad_clamp_fusion.1), kind=kCustom, calls=%fused_computation | custom fusion | bytes 4196352 | tf_op jit(solution)/shard_map/gather | solution.py:318
  59.8 4.1 %reshape.140 = bf16[128,1,4,2048]{3,2,0,1:T(4,128)(2,1)} reshape(bf16[512,2048]{1,0:T(8,128)(2,1)} %gather_fusion) | data formatting | bytes 4194304 | tf_op jit(solution)/shard_map/reshape | solution.py:319
  63.9 40.8 %all_to_all.10 = bf16[128,1,4,2048]{3,2,1,0:T(4,128)(2,1)S(1)} all-to-all(bf16[128,1,4,2048]{3,2,1,0:T(4,128)(2,1)} %bitcast.100), channel_id=1, replica_groups=mesh['sp'=16,'dp'=8] {'sp','dp'}, dimensions={0} | all-to-all | bytes 4194304 | tf_op jit(solution)/shard_map/all_to_all | solution.py:321
  104.8 1.3 copy-done.1
  106.1 0.0 copy-done.5
  106.1 3.4 %fusion.10 = f32[128,1,4,512]{3,0,2,1:T(8,128)} fusion(bf16[1,2048,512]{2,1,0:T(8,128)(2,1)S(1)} %copy-done.5, bf16[128,1,4,2048]{3,2,1,0:T(4,128)(2,1)S(1)} %all_to_all.10), kind=kOutput, calls=%fused_computation.15 | convolution fusion | flops 1073741824 | bytes 5242880 | tf_op jit(solution)/shard_map/nesd,edf->nesf/dot_general | solution.py:269
  109.5 0.0 copy-done
  109.5 7.5 %fusion = bf16[128,1,4,2048]{3,0,2,1:T(8,128)(2,1)} fusion(bf16[1,512,2048]{2,1,0:T(8,128)(2,1)S(1)} %copy-done, bf16[1,2048,512]{2,1,0:T(8,128)(2,1)} %param.29, bf16[128,1,4,2048]{3,2,1,0:T(4,128)(2,1)} %copy-done.1, f32[128,1,4,512]{3,0,2,1:T(8,128)} %fusion.10), kind=kOutput, calls=%fused_computation.4 | convolution fusion | flops 2150105088 | bytes 9437184 | tf_op jit(solution)/shard_map/nesf,efd->nesd/dot_general | solution.py:272
  117.0 4.5 %copy.34 = bf16[128,1,4,2048]{3,2,1,0:T(4,128)(2,1)} copy(bf16[128,1,4,2048]{3,0,2,1:T(8,128)(2,1)} %fusion) | data formatting | bytes 4194304 | tf_op jit(solution)/shard_map/convert_element_type | solution.py:274
  121.5 5.9 %all-to-all-start.1 = ((bf16[128,1,4,2048]{3,2,1,0:T(4,128)(2,1)}), bf16[128,1,4,2048]{3,2,1,0:T(4,128)(2,1)}, u32[]{:S(2)}, u32[]{:S(2)}) async-start(bf16[128,1,4,2048]{3,2,1,0:T(4,128)(2,1)} %copy.34), calls=%async_computation.1 | async-start | bytes 4194304 | tf_op jit(solution)/shard_map/all_to_all | solution.py:326
  127.4 0.0 copy-done.3
  127.5 0.0 copy-done.4
  127.5 0.1 copy.26
  127.6 29.7 %all-to-all-done.1 = bf16[128,1,4,2048]{3,2,1,0:T(4,128)(2,1)} async-done(((bf16[128,1,4,2048]{3,2,1,0:T(4,128)(2,1)}), bf16[128,1,4,2048]{3,2,1,0:T(4,128)(2,1)}, u32[]{:S(2)}, u32[]{:S(2)}) %all-to-all-start.1) | async-done | bytes 2097184 | tf_op jit(solution)/shard_map/all_to_all | solution.py:326
  157.3 4.0 %reshape.146 = bf16[512,2048]{1,0:T(8,128)(2,1)} reshape(bf16[128,1,4,2048]{3,2,1,0:T(4,128)(2,1)} %all-to-all-done.1) | data formatting | bytes 4194304 | tf_op jit(solution)/shard_map/reshape | solution.py:328
  161.3 4.2 %gather_fusion.1 = bf16[256,2048]{1,0:T(8,128)(2,1)S(1)} fusion(bf16[512,2048]{1,0:T(8,128)(2,1)} %reshape.146, s32[1024]{0:T(1024)S(1)} %pad_clamp_fusion), kind=kCustom, calls=%fused_computation.1 | custom fusion | bytes 2098176 | tf_op jit(solution)/shard_map/gather | solution.py:328
  165.5 2.4 %reshape.148 = f32[128,2,2048]{2,1,0:T(2,128)} reshape(bf16[256,2048]{1,0:T(8,128)(2,1)S(1)} %gather_fusion.1) | data formatting | bytes 3145728 | tf_op jit(solution)/shard_map/convert_element_type | solution.py:329
  167.9 4.9 %multiply_reduce_fusion = f32[128,2048]{1,0:T(8,128)S(1)} fusion(f32[128,2,2048]{2,1,0:T(2,128)} %reshape.148, f32[128,2]{1,0:T(8,128)S(1)} %copy.26), kind=kLoop, calls=%fused_computation.12 | loop fusion | flops 786432 | bytes 3146752 | tf_op jit(solution)/shard_map/reduce_sum | solution.py:334
  172.8 0.9 fusion.39
  (19 shorter events, 0.1 us)
Async XLA Ops:
  0.0 109.5 %copy-start = (bf16[1,512,2048]{2,1,0:T(8,128)(2,1)S(1)}, bf16[1,512,2048]{2,1,0:T(8,128)(2,1)}, u32[]{:S(2)}) copy-start(bf16[1,512,2048]{2,1,0:T(8,128)(2,1)} %param.30) | copy-start | bytes 6291460
  63.9 42.1 %copy-start.5 = (bf16[1,2048,512]{2,1,0:T(8,128)(2,1)S(1)}, bf16[1,2048,512]{2,1,0:T(8,128)(2,1)}, u32[]{:S(2)}) copy-start(bf16[1,2048,512]{2,1,0:T(8,128)(2,1)} %param.28) | copy-start | bytes 6291460
  104.8 1.3 copy-start.1
  121.5 6.0 %copy-start.3 = (f32[1,128]{1,0:T(1,128)S(1)}, f32[1,128]{1,0:T(1,128)}, u32[]{:S(2)}) copy-start(f32[1,128]{1,0:T(1,128)} %param.27) | copy-start | bytes 1540
  121.5 6.0 %copy-start.4 = (f32[1,128]{1,0:T(1,128)S(1)}, f32[1,128]{1,0:T(1,128)}, u32[]{:S(2)}) copy-start(f32[1,128]{1,0:T(1,128)} %param.26) | copy-start | bytes 1540
  121.5 35.8 %all-to-all-start.1 = ((bf16[128,1,4,2048]{3,2,1,0:T(4,128)(2,1)}), bf16[128,1,4,2048]{3,2,1,0:T(4,128)(2,1)}, u32[]{:S(2)}, u32[]{:S(2)}) async-start(bf16[128,1,4,2048]{3,2,1,0:T(4,128)(2,1)} %copy.34), calls=%async_computation.1 | async-start | bytes 4194304 | tf_op jit(solution)/shard_map/all_to_all | solution.py:326
  167.9 4.9 %copy-start.2 = (bf16[128,2048]{1,0:T(8,128)(2,1)S(1)}, bf16[128,2048]{1,0:T(8,128)(2,1)}, u32[]{:S(2)}) copy-start(bf16[128,2048]{1,0:T(8,128)(2,1)} %get-tuple-element.7) | copy-start | bytes 1572868

commit v2 on v1

--- a/solution.py
+++ b/solution.py
@@ -1,5 +1,3 @@
-import functools
-
 import jax
 import jax.numpy as jnp
 import numpy as np
@@ -265,13 +263,397 @@
     )
 
 
-def expert_ffn(arrived, gate_weight, up_weight, down_weight):
-    gated = jnp.einsum("nesd,edf->nesf", arrived, gate_weight, preferred_element_type=jnp.float32)
-    lifted = jnp.einsum("nesd,edf->nesf", arrived, up_weight, preferred_element_type=jnp.float32)
-    hidden = (jax.nn.silu(gated) * lifted).astype(jnp.bfloat16)
-    return jnp.einsum(
-        "nesf,efd->nesd", hidden, down_weight, preferred_element_type=jnp.float32
-    ).astype(jnp.bfloat16)
+class Exchange:
+    def __init__(self, send_sem, recv_sem):
+        self.send_sem, self.recv_sem, self.copies = send_sem, recv_sem, {}
+
+    def start(self, name, src, dst, peer):
+        i = len(self.copies)
+        copy = pltpu.make_async_remote_copy(
+            src_ref=src,
+            dst_ref=dst,
+            send_sem=self.send_sem.at[i],
+            recv_sem=self.recv_sem.at[i],
+            device_id=peer,
+            device_id_type=MESH,
+        )
+        assert name not in self.copies
+        self.copies[name] = copy
+        copy.start()
+
+    def arrived(self, name):
+        self.copies[name].wait_recv()
+
+    def finish(self):
+        for copy in self.copies.values():
+            copy.wait_send()
+
+
+CHUNKS = 2
+
+
+def flat(ref, cols, lead):
+    block = ref[lead + (slice(None),) * (len(ref.shape) - len(lead) - 1) + (cols,)]
+    return block.reshape(-1, block.shape[-1])
+
+
+def expert_kernel(
+    normed_ref, ids_ref, gw_ref, fs_ref, stream_hbm, gate_hbm, up_hbm, down_hbm,
+    out_ref,
+    stream, gate, up, down, meta,
+    zs, rows, zrel, xs, xr, xrel, yr, yrel, gates, lifts, hidden,
+    made, back, backrel, ret, retrel, comb, zret, zretrel,
+    spread, pick1, pick2, home,
+    local_sem, send_sem, recv_sem,
+):
+    z, x, y, c = position()
+    width = normed_ref.shape[1]
+    step = width // CHUNKS
+    ring = {
+        "z": (at(z + 1, x, y, c), at(z - 1, x, y, c)),
+        "x": (at(z, x + 1, y, c), at(z, x - 1, y, c)),
+        "y": (at(z, x, y + 1, c), at(z, x, y - 1, c)),
+        "yc": (at(z, x, y + 1, 1 - c), at(z, x, y - 1, 1 - c)),
+    }
+    across, twin = at(z + 2, x, y, c), at(z, x, y, 1 - c)
+
+    loads = []
+    for i, (src, dst) in enumerate(
+        [(gate_hbm.at[0], gate), (up_hbm.at[0], up), (down_hbm.at[0], down), (stream_hbm, stream)]
+    ):
+        load = pltpu.make_async_copy(src, dst, local_sem.at[i])
+        load.start()
+        loads.append(load)
+
+    barrier = pltpu.get_barrier_semaphore()
+    peers = [p for pair in ring.values() for p in pair] + [across, twin]
+    for peer in peers:
+        pl.semaphore_signal(barrier, inc=1, device_id=peer, device_id_type=MESH)
+
+    ex = Exchange(send_sem, recv_sem)
+
+    def iota(shape, dim):
+        return lax.broadcasted_iota(jnp.int32, shape, dim)
+
+    eye = iota((128, 128), 0) == iota((128, 128), 1)
+    earlier = (iota((128, 128), 0) < iota((128, 128), 1)).astype(F32)
+
+    def lay(column):
+        return jnp.sum(jnp.where(eye, column, 0.0), axis=0, keepdims=True)
+
+    def stand(row):
+        return jnp.sum(jnp.where(eye, row, 0.0), axis=1, keepdims=True)
+
+    def counted(members):
+        return jnp.dot(members, earlier, preferred_element_type=F32)
+
+    ids = ids_ref[...].astype(F32)
+    meta[0, 0:1, :] = lay(ids[:, 0:1])
+    meta[0, 1:2, :] = lay(ids[:, 1:2])
+    meta[0, 2:3, :] = gw_ref[...]
+    meta[0, 3:4, :] = fs_ref[...]
+    meta[0, 4:8, :] = jnp.zeros((4, 128), F32)
+
+    pl.semaphore_wait(barrier, len(peers))
+    ex.start("meta+", meta.at[0], meta.at[3], ring["z"][0])
+    ex.start("meta-", meta.at[0], meta.at[1], ring["z"][1])
+    ex.start("meta2", meta.at[0], meta.at[2], across)
+
+    relative = ((meta[0, 0:1, :].astype(jnp.int32) >> 5) - z + 4) & 3
+    members = (iota((8, 128), 0) == relative).astype(F32)
+    rank = jnp.sum(members * counted(members), axis=0, keepdims=True)
+    target = relative.astype(F32) * 32.0 + rank
+    pack = (iota((128, 128), 0).astype(F32) == target).astype(BF16)
+    home[...] = (iota((128, 128), 1).astype(F32) == stand(target)).astype(BF16)
+
+    def chunk(i):
+        return pl.ds(i * step, step)
+
+    def halves(ref, key, cols):
+        return ref.at[key + (pl.ds(0, 16), cols)], ref.at[key + (pl.ds(16, 16), cols)]
+
+    def ring_send(tag, axis, i, opposite, relays, direct):
+        plus, minus = ring[axis]
+        ex.start((tag, "out+", i), opposite[0], relays[0], plus)
+        ex.start((tag, "out-", i), opposite[1], relays[1], minus)
+        ex.start((tag, "+", i), direct[0][0], direct[0][1], plus)
+        ex.start((tag, "-", i), direct[1][0], direct[1][1], minus)
+
+    def ring_forward(tag, axis, i, relays, finals):
+        plus, minus = ring[axis]
+        ex.arrived((tag, "out+", i))
+        ex.start((tag, "on+", i), relays[0], finals[0], plus)
+        ex.arrived((tag, "out-", i))
+        ex.start((tag, "on-", i), relays[1], finals[1], minus)
+
+    def z_out(i, src, dst, relay):
+        cols = chunk(i)
+        relays = relay.at[0, :, cols], relay.at[1, :, cols]
+        ring_send(
+            ("z", id_of(src)), "z", i, halves(src, (2,), cols), relays,
+            (
+                (src.at[1, :, cols], dst.at[3, :, cols]),
+                (src.at[3, :, cols], dst.at[1, :, cols]),
+            ),
+        )
+
+    def id_of(ref):
+        return "d" if ref is zs else "r"
+
+    def z_on(i, src, dst, relay):
+        cols = chunk(i)
+        relays = relay.at[0, :, cols], relay.at[1, :, cols]
+        ring_forward(("z", id_of(src)), "z", i, relays, halves(dst, (2,), cols))
+
+    def z_in(i, src):
+        for sign in ("+", "-", "on+", "on-"):
+            ex.arrived((("z", id_of(src)), sign, i))
+
+    for i in range(CHUNKS):
+        cols = chunk(i)
+        packed = jnp.dot(pack, normed_ref[:, cols], preferred_element_type=F32).astype(BF16)
+        zs[:, :, cols] = packed.reshape(4, 32, step)
+        rows[0, :, cols] = packed[0:32]
+        z_out(i, zs, rows, zrel)
+
+    for name in ("meta+", "meta-", "meta2"):
+        ex.arrived(name)
+    stacks = [[], [], [], []]
+    for r in range(4):
+        first = meta[r, 0:1, :]
+        inside = (first.astype(jnp.int32) >> 5) == z
+        members = jnp.broadcast_to(inside.astype(F32), (8, 128))
+        rank = counted(members)[0:1]
+        places = jnp.where(inside, rank, -1.0)
+        taken = iota((32, 128), 0).astype(F32) == places
+        for which in range(4):
+            stacks[which].append(
+                jnp.sum(
+                    jnp.where(taken, meta[r, which : which + 1, :], 0.0), axis=1, keepdims=True
+                )
+            )
+    first, second, group_share, first_share = [jnp.concatenate(s, axis=0) for s in stacks]
+
+    def relative_expert(column):
+        e = lay(column).astype(jnp.int32) & 31
+        return ((((e >> 3) - x + 4) & 3) << 3) + (((((e >> 1) & 3) - y + 4) & 3) << 1) + (
+            (e & 1) ^ c
+        )
+
+    rel1, rel2 = relative_expert(first), relative_expert(second)
+    named1 = (iota((32, 128), 0) == rel1).astype(F32)
+    named2 = (iota((32, 128), 0) == rel2).astype(F32)
+    ahead = counted(named1 + named2)
+    slot1 = rel1.astype(F32) * 16.0 + jnp.sum(named1 * ahead, axis=0, keepdims=True)
+    slot2 = rel2.astype(F32) * 16.0 + jnp.sum(named2 * ahead, axis=0, keepdims=True)
+    places = iota((512, 128), 0).astype(F32)
+    spread[...] = ((places == slot1) | (places == slot2)).astype(BF16)
+    places = iota((128, 512), 1).astype(F32)
+    pick1[...] = (places == stand(slot1)).astype(BF16)
+    pick2[...] = (places == stand(slot2)).astype(BF16)
+    weight1 = group_share * first_share
+    weight2 = group_share * (1.0 - first_share)
+
+    def x_parts(i, relay, dst):
+        cols = chunk(i)
+        relays = relay.at[0, :, :, :, cols], relay.at[1, :, :, :, cols]
+        finals = dst.at[2, pl.ds(0, 2), :, :, cols], dst.at[2, pl.ds(2, 2), :, :, cols]
+        return relays, finals
+
+    def x_out(tag, i, src, dst, relay):
+        cols = chunk(i)
+        relays, _ = x_parts(i, relay, dst)
+        ring_send(
+            (tag, "x"), "x", i,
+            (src.at[2, pl.ds(0, 2), :, :, cols], src.at[2, pl.ds(2, 2), :, :, cols]), relays,
+            (
+                (src.at[1, :, :, :, cols], dst.at[3, :, :, :, cols]),
+                (src.at[3, :, :, :, cols], dst.at[1, :, :, :, cols]),
+            ),
+        )
+
+    def x_on(tag, i, dst, relay):
+        relays, finals = x_parts(i, relay, dst)
+        ring_forward((tag, "x"), "x", i, relays, finals)
+
+    def y_out(tag, i, r, src, dst, relay):
+        name = (tag, "y", r)
+        ring_send(
+            name, "y", i, (src(2, 0), src(2, 1)), (relay.at[0, r, :, chunk(i)], relay.at[1, r, :, chunk(i)]),
+            ((src(1, 0), dst(3, 0)), (src(3, 0), dst(1, 0))),
+        )
+        ex.start((name, "c+", i), src(1, 1), dst(3, 1), ring["yc"][0])
+        ex.start((name, "c-", i), src(3, 1), dst(1, 1), ring["yc"][1])
+        ex.start((name, "twin", i), src(0, 1), dst(0, 1), twin)
+
+    def y_on(tag, i, r, dst, relay):
+        name = (tag, "y", r)
+        ex.arrived((name, "out+", i))
+        ex.start((name, "on+", i), relay.at[0, r, :, chunk(i)], dst(2, 0), ring["y"][0])
+        ex.arrived((name, "out-", i))
+        ex.start((name, "on-", i), relay.at[1, r, :, chunk(i)], dst(2, 1), ring["yc"][1])
+
+    def y_in(tag, i, r):
+        for sign in ("+", "-", "c+", "c-", "twin", "on+", "on-"):
+            ex.arrived(((tag, "y", r), sign, i))
+
+    def block(ref, r, cols):
+        return lambda ry, rc: ref.at[r, ry, rc, :, cols]
+
+    def to_expert(i, r):
+        cols = chunk(i)
+        source = xs if r == 0 else xr
+        y_out("d", i, r, block(source, r, cols), block(yr, r, cols), yrel)
+        yr[r, 0, 0, :, cols] = source[r, 0, 0, :, cols]
+
+    for i in range(CHUNKS):
+        cols = chunk(i)
+        z_on(i, zs, rows, zrel)
+        z_in(i, zs)
+        slots = jnp.dot(
+            spread[...], rows[:, :, cols].reshape(128, step), preferred_element_type=F32
+        )
+        xs[:, :, :, :, cols] = slots.astype(BF16).reshape(4, 4, 2, 16, step)
+        x_out("d", i, xs, xr, xrel)
+        to_expert(i, 0)
+        x_on("d", i, xr, xrel)
+
+    loads[0].wait()
+    loads[1].wait()
+    for i in range(CHUNKS):
+        cols = chunk(i)
+        y_on("d", i, 0, block(yr, 0, cols), yrel)
+        ex.arrived((("d", "x"), "+", i))
+        to_expert(i, 3)
+        ex.arrived((("d", "x"), "-", i))
+        to_expert(i, 1)
+        y_on("d", i, 3, block(yr, 3, cols), yrel)
+        y_on("d", i, 1, block(yr, 1, cols), yrel)
+        ex.arrived((("d", "x"), "on+", i))
+        ex.arrived((("d", "x"), "on-", i))
+        to_expert(i, 2)
+        y_on("d", i, 2, block(yr, 2, cols), yrel)
+        for r in range(4):
+            y_in("d", i, r)
+        arrived = yr[:, :, :, :, cols].reshape(512, step)
+        for total, weight in ((gates, gate), (lifts, up)):
+            product = jnp.dot(arrived, weight[cols, :], preferred_element_type=F32)
+            total[...] = product if i == 0 else total[...] + product
+
+    g = gates[...]
+    hidden[...] = (g / (1.0 + jnp.exp(-g)) * lifts[...]).astype(BF16)
+    loads[2].wait()
+
+    def landing(r, cols):
+        return block(ret if r == 0 else back, r, cols)
+
+    def x_back_parts(i):
+        cols = chunk(i)
+        relays = retrel.at[0, :, :, :, cols], retrel.at[1, :, :, :, cols]
+        finals = ret.at[2, pl.ds(0, 2), :, :, cols], ret.at[2, pl.ds(2, 2), :, :, cols]
+        return relays, finals
+
+    for i in range(CHUNKS):
+        cols = chunk(i)
+        produced = jnp.dot(hidden[...], down[:, cols], preferred_element_type=F32)
+        made[:, :, :, :, cols] = produced.astype(BF16).reshape(4, 4, 2, 16, step)
+        for r in (2, 3, 1, 0):
+            y_out("r", i, r, block(made, r, cols), landing(r, cols), backrel)
+            (ret if r == 0 else back)[r, 0, 0, :, cols] = made[r, 0, 0, :, cols]
+
+    for i in range(CHUNKS):
+        cols = chunk(i)
+        relays, finals = x_back_parts(i)
+        plus, minus = ring["x"]
+        for r in (2, 3, 1, 0):
+            y_on("r", i, r, landing(r, cols), backrel)
+        y_in("r", i, 2)
+        ex.start(("r", "xout+", i), back.at[2, pl.ds(0, 2), :, :, cols], relays[0], plus)
+        ex.start(("r", "xout-", i), back.at[2, pl.ds(2, 2), :, :, cols], relays[1], minus)
+        y_in("r", i, 3)
+        ex.start(("r", "x-", i), back.at[3, :, :, :, cols], ret.at[1, :, :, :, cols], minus)
+        y_in("r", i, 1)
+        ex.start(("r", "x+", i), back.at[1, :, :, :, cols], ret.at[3, :, :, :, cols], plus)
+        ex.arrived(("r", "xout+", i))
+        ex.start(("r", "xon+", i), relays[0], finals[0], plus)
+        ex.arrived(("r", "xout-", i))
+        ex.start(("r", "xon-", i), relays[1], finals[1], minus)
+        y_in("r", i, 0)
+
+    for i in range(CHUNKS):
+        cols = chunk(i)
+        for sign in ("x+", "x-", "xon+", "xon-"):
+            ex.arrived(("r", sign, i))
+        returned = ret[:, :, :, :, cols].reshape(512, step)
+        one = jnp.dot(pick1[...], returned, preferred_element_type=F32)
+        two = jnp.dot(pick2[...], returned, preferred_element_type=F32)
+        mixed = (weight1 * one + weight2 * two).astype(BF16)
+        comb[:, :, cols] = mixed.reshape(4, 32, step)
+        zret[0, :, cols] = mixed[0:32]
+        z_out(i, comb, zret, zretrel)
+
+    loads[3].wait()
+    for i in range(CHUNKS):
+        cols = chunk(i)
+        z_on(i, comb, zret, zretrel)
+        z_in(i, comb)
+        added = jnp.dot(
+            home[...], zret[:, :, cols].reshape(128, step), preferred_element_type=F32
+        )
+        out_ref[:, cols] = (stream[:, cols].astype(F32) + added).astype(BF16)
+    ex.finish()
+
+
+def expert_layer(normed, ids, group_weight, first_share, stream, gate, up, down):
+    hbm = pl.BlockSpec(memory_space=pl.ANY)
+    vmem = pl.BlockSpec(memory_space=pltpu.VMEM)
+    tokens, width = normed.shape
+    _, _, ff = gate.shape
+    slots = (4, 4, 2, 16, width)
+    copies = 3 + 96 * CHUNKS
+    return pl.pallas_call(
+        expert_kernel,
+        out_shape=jax.ShapeDtypeStruct((tokens, width), BF16),
+        in_specs=[vmem] * 4 + [hbm] * 4,
+        out_specs=vmem,
+        scratch_shapes=[
+            pltpu.VMEM((tokens, width), BF16),
+            pltpu.VMEM((width, ff), BF16),
+            pltpu.VMEM((width, ff), BF16),
+            pltpu.VMEM((ff, width), BF16),
+            pltpu.VMEM((4, 8, 128), F32),
+            pltpu.VMEM((4, 32, width), BF16),
+            pltpu.VMEM((4, 32, width), BF16),
+            pltpu.VMEM((2, 16, width), BF16),
+            pltpu.VMEM(slots, BF16),
+            pltpu.VMEM(slots, BF16),
+            pltpu.VMEM((2, 2, 2, 16, width), BF16),
+            pltpu.VMEM(slots, BF16),
+            pltpu.VMEM((2, 4, 16, width), BF16),
+            pltpu.VMEM((512, ff), F32),
+            pltpu.VMEM((512, ff), F32),
+            pltpu.VMEM((512, ff), BF16),
+            pltpu.VMEM(slots, BF16),
+            pltpu.VMEM(slots, BF16),
+            pltpu.VMEM((2, 4, 16, width), BF16),
+            pltpu.VMEM(slots, BF16),
+            pltpu.VMEM((2, 2, 2, 16, width), BF16),
+            pltpu.VMEM((4, 32, width), BF16),
+            pltpu.VMEM((4, 32, width), BF16),
+            pltpu.VMEM((2, 16, width), BF16),
+            pltpu.VMEM((512, 128), BF16),
+            pltpu.VMEM((128, 512), BF16),
+            pltpu.VMEM((128, 512), BF16),
+            pltpu.VMEM((128, 128), BF16),
+            pltpu.SemaphoreType.DMA((4,)),
+            pltpu.SemaphoreType.DMA((copies,)),
+            pltpu.SemaphoreType.DMA((copies,)),
+        ],
+        compiler_params=pltpu.CompilerParams(
+            collective_id=1, has_side_effects=True, vmem_limit_bytes=60 * 1024 * 1024
+        ),
+        name="experts",
+    )(normed, ids, group_weight, first_share, stream, gate, up, down)
 
 
 def local(
@@ -291,50 +673,15 @@
     up_weight,
     down_weight,
 ):
-    sp_count = lax.axis_size("sp")
-    dp_count = lax.axis_size("dp")
-    tokens = query_proj.shape[1]
     stream, normed = attention(
         query_proj[0], key_proj[0], value_proj[0], out_weight, residual_in[0],
         query_gain, key_gain, post_gain, pre_gain,
     )
-    model_width = normed.shape[1]
-    local_experts = gate_weight.shape[0]
-    expert_count = local_experts * sp_count * dp_count
-    capacity = 4 * tokens // expert_count
-    chosen = route_ids.reshape(2 * tokens)
-    onehot = (chosen[:, None] == jnp.arange(expert_count, dtype=jnp.int32)[None, :]).astype(
-        jnp.int32
-    )
-    earlier = jnp.cumsum(onehot, axis=0) - onehot
-    slot_rank = jnp.sum(earlier * onehot, axis=1)
-    slot_index = chosen * capacity + slot_rank
-    source_row = (
-        jnp.full((expert_count * capacity,), tokens, jnp.int32)
-        .at[slot_index]
-        .set(jnp.arange(2 * tokens, dtype=jnp.int32) // 2)
-    )
-    padded = jnp.concatenate([normed, jnp.zeros((1, model_width), jnp.bfloat16)], axis=0)
-    outgoing = padded[source_row]
-    shaped = outgoing.reshape(sp_count * dp_count, local_experts, capacity, model_width)
-    answered = expert_ffn(
-        lax.all_to_all(shaped, ("sp", "dp"), split_axis=0, concat_axis=0, tiled=True),
-        gate_weight,
-        up_weight,
-        down_weight,
-    )
-    returned = lax.all_to_all(answered, ("sp", "dp"), split_axis=0, concat_axis=0, tiled=True)
-    results = (
-        returned.reshape(expert_count * capacity, model_width)[slot_index]
-        .astype(jnp.float32)
-        .reshape(tokens, 2, model_width)
-    )
-    share = first_share[0]
-    weight_pair = group_weight[0][:, None] * jnp.stack([share, 1.0 - share], axis=1)
-    combined = jnp.sum(weight_pair[:, :, None] * results, axis=1)
-    return (
-        (stream.astype(jnp.float32) + combined).astype(jnp.bfloat16).reshape(1, tokens, model_width)
-    )
+    out = expert_layer(
+        normed, route_ids[0], group_weight, first_share, stream,
+        gate_weight, up_weight, down_weight,
+    )
+    return out[None]
 
 
 def solution(mesh):

time: 174 us -> 175 us (level)
  Pallas kernels: 51.2 us -> 171 us
  blocking collectives: 40.8 us -> 0 us
  waiting for transfers between devices: 29.7 us -> 0 us
  local copies, waits for them, and re-layouts: 28 us -> 3.29 us
  matrix products: 10.9 us -> 0 us
  other arithmetic: 6.92 us -> 0 us
  starting transfers between devices: 5.94 us -> 0 us
    pallas_call x0 -> x1, Pallas kernels: none -> 119 us  [expert_layer(): pl.pallas_call(expert_kernel, out_shape=jax.ShapeDtypeStruct((tokens, wid...]
    all_to_all x1 -> x0, blocking collectives: 40.8 us -> none  [local(): lax.all_to_all(shaped, ('sp', 'dp'), split_axis=0, concat_axis=0, tiled=T...]
    all_to_all x1 -> x0, waiting for transfers between devices: 29.7 us -> none  [local(): lax.all_to_all(answered, ('sp', 'dp'), split_axis=0, concat_axis=0, tiled...]
    dot_general x2 -> x0, matrix products: 10.9 us -> none  [the longest x1 7.52 us: expert_ffn(): jnp.einsum('nesf,efd->nesd', hidden, down_weight, preferred_element_type=...]
    reshape x2 -> x0, local copies, waits for them, and re-layouts: 8.08 us -> none  [the longest x1 4.12 us: local(): outgoing.reshape(sp_count * dp_count, local_experts, capacity, model_width)]
    gather x2 -> x0, local copies, waits for them, and re-layouts: 7.57 us -> none  [the longest x1 4.22 us: local(): returned.reshape(expert_count * capacity, model_width)[slot_index]]
    convert_element_type x2 -> x0, local copies, waits for them, and re-layouts: 6.87 us -> none  [the longest x1 4.5 us: expert_ffn(): return jnp.einsum('nesf,efd->nesd', hidden, down_weight, preferred_elemen...]
    all_to_all x1 -> x0, starting transfers between devices: 5.94 us -> none  [local(): lax.all_to_all(answered, ('sp', 'dp'), split_axis=0, concat_axis=0, tiled...]
  transfers between devices with their start and end apart: 1 -> 0, of which waited for: 1 -> 0; matrix products, arithmetic and copies ran while one was open for 0% -> 0% of each run, Pallas kernels for 0% -> 0%
where the time goes in v2:
time: 175 us; the launch traced here: 174 us
  Pallas kernels  171 us (98%)
  local copies, waits for them, and re-layouts  3.29 us (2%)
    pallas_call x1, Pallas kernels, expert_layer(): pl.pallas_call(expert_kernel, out_shape=jax.ShapeDtypeStruct((tokens, wid...  119 us
    pallas_call x1, Pallas kernels, attention(): pl.pallas_call(attention_kernel, out_shape=[jax.ShapeDtypeStruct((tokens,...  51.3 us

profile of v2, /device:TPU:1, one launch (start us, length us, event | category | flops | bytes accessed | tf_op | source)
XLA Modules:
  0.0 173.8 jit_solution(5130367250192215035)
XLA Ops:
  0.0 1.4 copy.17
  1.4 51.3 %attention.1 = (bf16[128,2048]{1,0:T(8,128)(2,1)}, bf16[128,2048]{1,0:T(8,128)(2,1)}) custom-call(bf16[128,2048]{1,0:T(8,128)(2,1)} %bitcast.11, bf16[128,512]{1,0:T(8,128)(2,1)} %bitcast.14, bf16[128,512]{1,0:T(8,128)(2,1)} %bitcast.15, bf16[2048,2048]{1,0:T(8,128)(2,1)} %w_hbm.1, bf16[128,2048]{1,0:T(8,128)(2,1)} %bitcast.12, ...), custom_call_target="tpu_custom_call" | custom-call | tf_op jit(solution)/shard_map/attention/pallas_call | solution.py:234
  52.7 119.3 %experts.1 = bf16[128,2048]{1,0:T(8,128)(2,1)} custom-call(bf16[128,2048]{1,0:T(8,128)(2,1)} %get-tuple-element.7.normed_ref, s32[128,2]{1,0:T(8,128)} %bitcast.13, f32[1,128]{1,0:T(1,128)} %gw_ref.1, f32[1,128]{1,0:T(1,128)} %fs_ref.1, bf16[128,2048]{1,0:T(8,128)(2,1)} %get-tuple-element.8.stream_hbm, bf16[1,2048,512]{2,1,0:T(8,128)(2,1)} %gate_hbm.1, ...), custom_call_target="tpu_custom_call" | custom-call | tf_op jit(solution)/shard_map/experts/pallas_call | solution.py:614
  171.9 1.9 %copy.19 = bf16[1,128,2048]{2,1,0:T(8,128)(2,1)} copy(bf16[1,128,2048]{2,1,0:T(8,128)(2,1)} %bitcast.10) | data formatting | bytes 1048576

commit v3 on v1

v3 whole, which is shorter than its diff:
```python
import jax
import jax.numpy as jnp
import numpy as np
from jax import lax
from jax.experimental import pallas as pl
from jax.experimental.pallas import tpu as pltpu
from jax.sharding import PartitionSpec as P

HEADS = 16
KV_HEADS = 4
HEAD_DIM = 128
GRID_W = 64
RING = 4
EPSILON = 1e-06
MESH = pl.DeviceIdType.MESH


class Phase:
    def __init__(self):
        self.scope = None

    def __call__(self, name=None):
        if self.scope is not None:
            self.scope.__exit__(None, None, None)
        self.scope = None
        if name is not None:
            self.scope = jax.named_scope(name)
            self.scope.__enter__()


F32 = jnp.float32
BF16 = jnp.bfloat16


def angle_tables():
    quarter = HEAD_DIM // 4
    inverse = (np.float32(10000.0) ** (-np.arange(quarter, dtype=np.float32) / quarter)).astype(
        np.float32
    )
    places = np.concatenate([np.arange(32), np.arange(GRID_W)]).astype(np.float32)
    angles = places[:, None] * np.tile(inverse, 4)[None, :]
    return np.stack([np.cos(angles), np.sin(angles)]).astype(np.float32)


def position():
    s = lax.axis_index("sp")
    d = lax.axis_index("dp")
    return s // RING, s % RING, d // 2, d % 2


def at(z, x, y, c):
    return (
        ((z + 2 * RING) % RING) * RING + (x + 2 * RING) % RING,
        ((y + 2 * RING) % RING) * 2 + c,
    )


def turn(heads, gain, cos, sin):
    normed = (
        heads * lax.rsqrt(jnp.mean(heads * heads, axis=-1, keepdims=True) + EPSILON) * gain
    )
    lane = lax.broadcasted_iota(jnp.int32, normed.shape, 1)
    turned = jnp.where(
        (lane // 32) % 2 == 0, -pltpu.roll(normed, 96, 1), pltpu.roll(normed, 32, 1)
    )
    return (normed * cos + turned * sin).astype(BF16)


class Exchange:
    def __init__(self, send_sem, recv_sem):
        self.send_sem, self.recv_sem, self.copies = send_sem, recv_sem, {}

    def start(self, name, src, dst, peer):
        i = len(self.copies)
        copy = pltpu.make_async_remote_copy(
            src_ref=src,
            dst_ref=dst,
            send_sem=self.send_sem.at[i],
            recv_sem=self.recv_sem.at[i],
            device_id=peer,
            device_id_type=MESH,
        )
        assert name not in self.copies
        self.copies[name] = copy
        copy.start()

    def arrived(self, *names):
        for name in names:
            self.copies[name].wait_recv()

    def finish(self):
        for copy in self.copies.values():
            copy.wait_send()


ROUNDS = 2
COPIES = 40 + 3 + ROUNDS * (2 * 84 + 2 * 6)


def iota(shape, dim):
    return lax.broadcasted_iota(jnp.int32, shape, dim)


def layer_kernel(
    q_hbm, k_hbm, v_hbm, w_hbm, res_hbm, gate_hbm, up_hbm, down_hbm,
    table_ref, qg_ref, kg_ref, postg_ref, preg_ref, ids_ref, gw_ref, fs_ref,
    out_ref,
    kv, qt, q_raw, k_raw, v_raw, w, res, top, total, acc, att, mixed, normed,
    gate, up, down, meta,
    zs, rows, zrel, xs, xr, xrel, yr, yrel, gates, lifts, hidden,
    made, back, backrel, ret, retrel, comb, zret, zretrel,
    spread, pick1, pick2, home,
    local_sem, send_sem, recv_sem,
):
    z, x, y, c = position()
    width = q_raw.shape[1]
    phase = Phase()
    phase("turn")
    loads = {}
    for i, (name, src, dst) in enumerate(
        [
            ("k", k_hbm, k_raw), ("v", v_hbm, v_raw), ("q", q_hbm, q_raw), ("res", res_hbm, res),
            ("w", w_hbm, w), ("gate", gate_hbm.at[0], gate), ("up", up_hbm.at[0], up),
            ("down", down_hbm.at[0], down),
        ]
    ):
        loads[name] = pltpu.make_async_copy(src, dst, local_sem.at[i])
        loads[name].start()

    ring = {
        "z": (at(z + 1, x, y, c), at(z - 1, x, y, c)),
        "x": (at(z, x + 1, y, c), at(z, x - 1, y, c)),
        "y": (at(z, x, y + 1, c), at(z, x, y - 1, c)),
        "yc": (at(z, x, y + 1, 1 - c), at(z, x, y - 1, 1 - c)),
    }
    across, twin = at(z + 2, x, y, c), at(z, x, y, 1 - c)
    barrier = pltpu.get_barrier_semaphore()
    peers = [p for pair in ring.values() for p in pair] + [across, twin]
    for peer in peers:
        pl.semaphore_signal(barrier, inc=1, device_id=peer, device_id_type=MESH)
    ex = Exchange(send_sem, recv_sem)

    lane = iota((GRID_W, HEAD_DIM), 1)

    def table(which):
        halves = []
        for part in range(2):
            row = table_ref[which, pl.ds(2 * (z * RING + x) + part, 1), :]
            halves.append(jnp.where(lane < 64, row, table_ref[which, 32 : 32 + GRID_W, :]))
        return jnp.concatenate(halves, axis=0)

    cos, sin = table(0), table(1)
    meta[0, 0:2, :] = ids_ref[...].astype(F32)
    meta[0, 2:3, :] = gw_ref[...]
    meta[0, 3:4, :] = fs_ref[...]
    meta[0, 4:8, :] = jnp.zeros((4, 128), F32)
    loads["k"].wait()
    for h in range(KV_HEADS):
        raw = k_raw[:, h * 128 : (h + 1) * 128].astype(F32)
        kv[h // 2, 0, 0, :, (h % 2) * 128 : (h % 2 + 1) * 128] = turn(raw, kg_ref[...], cos, sin)
    loads["v"].wait()
    for half in range(2):
        kv[half, 0, 0, :, 256:512] = v_raw[:, half * 256 : (half + 1) * 256]
    phase("barrier")
    pl.semaphore_wait(barrier, len(peers))

    phase("start")
    first = ("x", "z")
    second = ("z", "x")
    low, high = pl.ds(0, 64), pl.ds(64, 64)

    def both(p, kind, r=0):
        names = ((kind, p, r, "+"), (kind, p, r, "-"))
        if kind == "own":
            peer = ring[first[p]]
            pairs = (kv.at[p, 0, 0], kv.at[p, 0, 3]), (kv.at[p, 0, 0], kv.at[p, 0, 1])
        elif kind == "relay":
            peer = ring[first[p]]
            pairs = (
                (kv.at[p, 0, 3, low], kv.at[p, 0, 2, low]),
                (kv.at[p, 0, 1, high], kv.at[p, 0, 2, high]),
            )
        elif kind == "far":
            peer = ring[second[p]]
            pairs = (kv.at[p, 0, r], kv.at[p, 3, r]), (kv.at[p, 0, r], kv.at[p, 1, r])
        else:
            peer = ring[second[p]]
            pairs = (
                (kv.at[p, 3, r, low], kv.at[p, 2, r, low]),
                (kv.at[p, 1, r, high], kv.at[p, 2, r, high]),
            )
        for name, (src, dst), to in zip(names, pairs, peer):
            ex.start(name, src, dst, to)

    def got(p, kind, r=0):
        ex.arrived((kind, p, r, "+"), (kind, p, r, "-"))

    for p in range(2):
        both(p, "own")
    for p in range(2):
        both(p, "far", 0)
    ex.start("meta+", meta.at[0], meta.at[3], ring["z"][0])
    ex.start("meta-", meta.at[0], meta.at[1], ring["z"][1])
    ex.start("meta2", meta.at[0], meta.at[2], across)

    phase("qturn")
    loads["q"].wait()
    for h in range(HEADS):
        raw = q_raw[:, h * 128 : (h + 1) * 128].astype(F32)
        qt[h // 4, (h % 4) * 128 : (h % 4 + 1) * 128, :] = turn(raw, qg_ref[...], cos, sin)

    phase("own")
    for p in range(2):
        got(p, "own")
        both(p, "relay")
    for r in (3, 1):
        for p in range(2):
            both(p, "far", r)

    phase("tables")
    eye = iota((128, 128), 0) == iota((128, 128), 1)
    earlier = (iota((128, 128), 0) < iota((128, 128), 1)).astype(F32)

    def lay(column):
        return jnp.sum(jnp.where(eye, column, 0.0), axis=0, keepdims=True)

    def stand(row):
        return jnp.sum(jnp.where(eye, row, 0.0), axis=1, keepdims=True)

    def counted(members):
        return jnp.dot(members, earlier, preferred_element_type=F32)

    relative = ((meta[0, 0:1, :].astype(jnp.int32) >> 5) - z + 4) & 3
    members = (iota((8, 128), 0) == relative).astype(F32)
    rank = jnp.sum(members * counted(members), axis=0, keepdims=True)
    target = relative.astype(F32) * 32.0 + rank
    pack = (iota((128, 128), 0).astype(F32) == target).astype(BF16)
    home[...] = (iota((128, 128), 1).astype(F32) == stand(target)).astype(BF16)

    phase("relay")
    for p in range(2):
        got(p, "relay")
        both(p, "far", 2)
    for p in range(2):
        got(p, "far", 0)
        both(p, "last", 0)

    phase("tables2")
    ex.arrived("meta+", "meta-", "meta2")
    stacks = [[], [], [], []]
    for r in range(4):
        inside = (meta[r, 0:1, :].astype(jnp.int32) >> 5) == z
        members = jnp.broadcast_to(inside.astype(F32), (8, 128))
        places = jnp.where(inside, counted(members)[0:1], -1.0)
        taken = iota((32, 128), 0).astype(F32) == places
        for which in range(4):
            stacks[which].append(
                jnp.sum(
                    jnp.where(taken, meta[r, which : which + 1, :], 0.0), axis=1, keepdims=True
                )
            )
    expert1, expert2, group_share, first_share = [jnp.concatenate(s, axis=0) for s in stacks]

    def relative_expert(column):
        e = lay(column).astype(jnp.int32) & 31
        return (
            ((((e >> 3) - x + 4) & 3) << 3)
            + (((((e >> 1) & 3) - y + 4) & 3) << 1)
            + ((e & 1) ^ c)
        )

    rel1, rel2 = relative_expert(expert1), relative_expert(expert2)
    named1 = (iota((32, 128), 0) == rel1).astype(F32)
    named2 = (iota((32, 128), 0) == rel2).astype(F32)
    ahead = counted(named1 + named2)
    slot1 = rel1.astype(F32) * 16.0 + jnp.sum(named1 * ahead, axis=0, keepdims=True)
    slot2 = rel2.astype(F32) * 16.0 + jnp.sum(named2 * ahead, axis=0, keepdims=True)
    places = iota((512, 128), 0).astype(F32)
    spread[...] = ((places == slot1) | (places == slot2)).astype(BF16)
    places = iota((128, 512), 1).astype(F32)
    pick1[...] = (places == stand(slot1)).astype(BF16)
    pick2[...] = (places == stand(slot2)).astype(BF16)
    weight1 = group_share * first_share
    weight2 = group_share * (1.0 - first_share)

    scale = float(np.log2(np.e) / np.sqrt(HEAD_DIM))

    def attend(r, opening):
        def one(g, carry):
            p, h = g // 2, g % 2
            keys = kv[p, r, :, :, pl.ds(pl.multiple_of(h * 128, 128), 128)].reshape(512, 128)
            values = kv[p, r, :, :, pl.ds(pl.multiple_of(256 + h * 128, 128), 128)].reshape(
                512, 128
            )
            scores = lax.dot_general(
                keys, qt[g], (((1,), (1,)), ((), ())), preferred_element_type=F32
            )
            peak = jnp.max(scores, axis=0, keepdims=True)
            if not opening:
                before = top[g]
                peak = jnp.maximum(peak, before)
            weights = jnp.exp2((scores - peak) * scale)
            summed = jnp.sum(weights, axis=0, keepdims=True)
            out = lax.dot_general(
                values, weights.astype(BF16), (((0,), (0,)), ((), ())),
                preferred_element_type=F32,
            )
            if not opening:
                shrink = jnp.exp2((before - peak) * scale)
                summed += total[g] * shrink
                out += acc[g] * shrink
            top[g] = peak
            total[g] = summed
            acc[g] = out
            return carry

        lax.fori_loop(0, KV_HEADS, one, 0)

    phase("att0")
    attend(0, True)
    phase("far31")
    for r in (3, 1):
        for p in range(2):
            got(p, "far", r)
            both(p, "last", r)
    phase("far2")
    for p in range(2):
        got(p, "far", 2)
        both(p, "last", 2)
    phase("att3")
    attend(3, False)
    phase("att1")
    attend(1, False)
    phase("last")
    for r in (0, 3, 1, 2):
        for p in range(2):
            got(p, "last", r)
    phase("att2")
    attend(2, False)

    phase("div")
    for g in range(KV_HEADS):
        scaled = acc[g] / total[g]
        for h in range(4):
            head = g * 4 + h
            att[:, head * 128 : (head + 1) * 128] = (
                scaled[:, h * 128 : (h + 1) * 128].T.astype(BF16)
            )
    loads["res"].wait()
    loads["w"].wait()
    phase("proj")

    def project(n, carry):
        cols = pl.ds(pl.multiple_of(n * 512, 512), 512)
        mixed[:, cols] = jnp.dot(att[...], w[:, cols], preferred_element_type=F32).astype(BF16)
        return carry

    lax.fori_loop(0, 4, project, 0)
    phase("norm")

    def norm(n, carry):
        at_rows = pl.ds(pl.multiple_of(n * 32, 32), 32)
        m = mixed[at_rows, :].astype(F32)
        m = m * lax.rsqrt(jnp.mean(m * m, axis=-1, keepdims=True) + EPSILON) * postg_ref[...]
        stream = (res[at_rows, :].astype(F32) + m).astype(BF16)
        res[at_rows, :] = stream
        s = stream.astype(F32)
        s = s * lax.rsqrt(jnp.mean(s * s, axis=-1, keepdims=True) + EPSILON) * preg_ref[...]
        normed[at_rows, :] = s.astype(BF16)
        return carry

    lax.fori_loop(0, 4, norm, 0)

    span = width // ROUNDS
    step = span // 2

    def span_of(i):
        return pl.ds(i * span, span)

    def z_parts(tag, i, src, dst, relay):
        cols = span_of(i)
        top_rows, low_rows = pl.ds(0, 16), pl.ds(16, 16)
        relays = relay.at[0, :, cols], relay.at[1, :, cols]
        opposite = src.at[2, top_rows, cols], src.at[2, low_rows, cols]
        finals = dst.at[2, top_rows, cols], dst.at[2, low_rows, cols]
        return cols, relays, opposite, finals

    def z_out(tag, i, src, dst, relay):
        cols, relays, opposite, _ = z_parts(tag, i, src, dst, relay)
        ex.start((tag, "z", "out+", i), opposite[0], relays[0], ring["z"][0])
        ex.start((tag, "z", "out-", i), opposite[1], relays[1], ring["z"][1])

    def z_direct(tag, i, src, dst):
        cols = span_of(i)
        ex.start((tag, "z", "+", i), src.at[1, :, cols], dst.at[3, :, cols], ring["z"][0])
        ex.start((tag, "z", "-", i), src.at[3, :, cols], dst.at[1, :, cols], ring["z"][1])

    def z_on(tag, i, src, dst, relay):
        _, relays, _, finals = z_parts(tag, i, src, dst, relay)
        for sign, relayed, final, to in zip("+-", relays, finals, ring["z"]):
            ex.arrived((tag, "z", "out" + sign, i))
            ex.start((tag, "z", "on" + sign, i), relayed, final, to)

    def z_in(tag, i):
        ex.arrived(*[(tag, "z", kind, i) for kind in ("+", "-", "on+", "on-")])

    def swap(tag, i, src, mid, dst, x_relay, y_relay):
        a, b = pl.ds(i * span, step), pl.ds(i * span + step, step)

        def block(ref, r, cols):
            return lambda ry, rc: ref.at[r, ry, rc, :, cols]

        def x_relays(cols):
            return x_relay.at[0, :, :, :, cols], x_relay.at[1, :, :, :, cols]

        def x_split(ref, cols):
            return ref.at[2, pl.ds(0, 2), :, :, cols], ref.at[2, pl.ds(2, 2), :, :, cols]

        def x_out(w, ref, cols):
            for sign, part, relayed, to in zip("+-", x_split(ref, cols), x_relays(cols), ring["x"]):
                ex.start((tag, w, "x", "out" + sign, i), part, relayed, to)

        def x_plus(w, ref, to, cols):
            ex.start(
                (tag, w, "x", "+", i), ref.at[1, :, :, :, cols], to.at[3, :, :, :, cols],
                ring["x"][0],
            )

        def x_minus(w, ref, to, cols):
            ex.start(
                (tag, w, "x", "-", i), ref.at[3, :, :, :, cols], to.at[1, :, :, :, cols],
                ring["x"][1],
            )

        def x_on(w, to_ref, cols):
            finals = x_split(to_ref, cols)
            for sign, relayed, final, to in zip("+-", x_relays(cols), finals, ring["x"]):
                ex.arrived((tag, w, "x", "out" + sign, i))
                ex.start((tag, w, "x", "on" + sign, i), relayed, final, to)

        def y_names(w, r, kinds):
            return [(tag, w, "y", r, kind, i) for kind in kinds]

        def y_relays(r, cols):
            return y_relay.at[0, r, :, cols], y_relay.at[1, r, :, cols]

        def y_out(w, r, ref, cols):
            part = block(ref, r, cols)
            names = y_names(w, r, ("out+", "out-"))
            for rc, relayed in enumerate(y_relays(r, cols)):
                ex.start(names[rc], part(2, rc), relayed, ring["y"][rc])

        def y_direct(w, r, ref, to_ref, cols):
            part, final = block(ref, r, cols), block(to_ref, r, cols)
            names = y_names(w, r, ("+", "-", "c+", "c-", "twin"))
            ex.start(names[0], part(1, 0), final(3, 0), ring["y"][0])
            ex.start(names[1], part(3, 0), final(1, 0), ring["y"][1])
            ex.start(names[2], part(1, 1), final(3, 1), ring["yc"][0])
            ex.start(names[3], part(3, 1), final(1, 1), ring["yc"][1])
            ex.start(names[4], part(0, 1), final(0, 1), twin)
            to_ref[r, 0, 0, :, cols] = ref[r, 0, 0, :, cols]

        def y_on(w, r, to_ref, cols):
            final = block(to_ref, r, cols)
            outs, ons = y_names(w, r, ("out+", "out-")), y_names(w, r, ("on+", "on-"))
            ex.arrived(outs[0])
            ex.start(ons[0], y_relays(r, cols)[0], final(2, 0), ring["y"][0])
            ex.arrived(outs[1])
            ex.start(ons[1], y_relays(r, cols)[1], final(2, 1), ring["yc"][1])

        def y_in(w, r):
            ex.arrived(*y_names(w, r, ("+", "-", "c+", "c-", "twin", "on+", "on-")))

        def landing(r):
            return dst if r == 0 else mid

        def origin(r):
            return src if r == 0 else mid

        x_out("a", src, a)
        y_out("b", 2, src, b)
        y_out("b", 3, src, b)
        y_out("b", 1, src, b)
        x_plus("a", src, mid, a)
        x_minus("a", src, mid, a)
        y_direct("b", 2, src, mid, b)
        y_direct("b", 3, src, mid, b)
        y_direct("b", 1, src, mid, b)
        y_out("a", 0, src, a)
        y_out("b", 0, src, b)
        yield
        y_on("b", 2, mid, b)
        y_on("b", 3, mid, b)
        y_on("b", 1, mid, b)
        y_direct("a", 0, src, dst, a)
        y_direct("b", 0, src, dst, b)
        x_on("a", mid, a)
        yield
        y_on("a", 0, dst, a)
        y_on("b", 0, dst, b)
        y_in("b", 2)
        x_out("b", mid, b)
        ex.arrived((tag, "a", "x", "+", i))
        y_out("a", 3, mid, a)
        y_direct("a", 3, mid, dst, a)
        ex.arrived((tag, "a", "x", "-", i))
        y_out("a", 1, mid, a)
        y_direct("a", 1, mid, dst, a)
        y_in("b", 3)
        x_minus("b", mid, dst, b)
        y_in("b", 1)
        x_plus("b", mid, dst, b)
        yield
        ex.arrived((tag, "a", "x", "on+", i), (tag, "a", "x", "on-", i))
        y_out("a", 2, mid, a)
        y_direct("a", 2, mid, dst, a)
        y_on("a", 3, dst, a)
        y_on("a", 1, dst, a)
        x_on("b", dst, b)
        yield
        y_on("a", 2, dst, a)
        yield
        for r in range(4):
            y_in("a", r)
        y_in("b", 0)
        ex.arrived(*[(tag, "b", "x", kind, i) for kind in ("+", "-", "on+", "on-")])

    def run(steps, count):
        for _ in range(count):
            next(steps, None)

    phase("pack")
    for i in range(ROUNDS):
        cols = span_of(i)
        packed = jnp.dot(pack, normed[:, cols], preferred_element_type=F32).astype(BF16)
        zs[:, :, cols] = packed.reshape(4, 32, span)
        rows[0, :, cols] = packed[0:32]
        z_out("d", i, zs, rows, zrel)
        if i == 0:
            z_direct("d", 0, zs, rows)

    def slots(i):
        cols = span_of(i)
        z_in("d", i)
        phase("slots%d" % i)
        spaced = jnp.dot(
            spread[...], rows[:, :, cols].reshape(128, span), preferred_element_type=F32
        )
        xs[:, :, :, :, cols] = spaced.astype(BF16).reshape(4, 4, 2, 16, span)

    def lift(i):
        cols = span_of(i)
        arrived = yr[:, :, :, :, cols].reshape(512, span)
        for sums, weight in ((gates, gate), (lifts, up)):
            product = jnp.dot(arrived, weight[cols, :], preferred_element_type=F32)
            sums[...] = product if i == 0 else sums[...] + product

    def lower(i):
        cols = span_of(i)
        produced = jnp.dot(hidden[...], down[:, cols], preferred_element_type=F32)
        made[:, :, :, :, cols] = produced.astype(BF16).reshape(4, 4, 2, 16, span)

    def combine(i):
        cols = span_of(i)
        returned = ret[:, :, :, :, cols].reshape(512, span)
        one = jnp.dot(pick1[...], returned, preferred_element_type=F32)
        two = jnp.dot(pick2[...], returned, preferred_element_type=F32)
        summed = (weight1 * one + weight2 * two).astype(BF16)
        comb[:, :, cols] = summed.reshape(4, 32, span)
        zret[0, :, cols] = summed[0:32]
        z_out("r", i, comb, zret, zretrel)
        z_direct("r", i, comb, zret)

    there = [swap("d", i, xs, xr, yr, xrel, yrel) for i in range(ROUNDS)]
    phase("zon0")
    z_on("d", 0, zs, rows, zrel)
    z_direct("d", 1, zs, rows)
    phase("zin0")
    slots(0)
    phase("d0_start")
    run(there[0], 1)
    phase("d0_b")
    run(there[0], 1)
    phase("zon1")
    z_on("d", 1, zs, rows, zrel)
    phase("d0_c")
    run(there[0], 1)
    phase("zin1")
    slots(1)
    phase("d0_d")
    run(there[0], 1)
    phase("d1_start")
    run(there[1], 1)
    phase("d0_e")
    run(there[0], 1)
    phase("d1_b")
    run(there[1], 1)
    phase("d0_in")
    run(there[0], 1)
    phase("lift0")
    loads["gate"].wait()
    loads["up"].wait()
    lift(0)
    for n in "cdef":
        phase("d1_" + n)
        run(there[1], 1)
    phase("lift1")
    lift(1)
    phase("silu")
    g = gates[...]
    hidden[...] = (g / (1.0 + jnp.exp(-g)) * lifts[...]).astype(BF16)
    loads["down"].wait()

    home_way = [swap("r", i, made, back, ret, retrel, backrel) for i in range(ROUNDS)]
    phase("lower0")
    lower(0)
    phase("r0_start")
    run(home_way[0], 1)
    phase("lower1")
    lower(1)
    for n in "bcd":
        phase("r0_" + n)
        run(home_way[0], 1)
    phase("r1_start")
    run(home_way[1], 1)
    phase("r0_e")
    run(home_way[0], 1)
    phase("r1_b")
    run(home_way[1], 1)
    phase("r0_in")
    run(home_way[0], 1)
    phase("combine0")
    combine(0)
    for n in "cd":
        phase("r1_" + n)
        run(home_way[1], 1)
    phase("zon0r")
    z_on("r", 0, comb, zret, zretrel)
    for n in "ef":
        phase("r1_" + n)
        run(home_way[1], 1)
    phase("combine1")
    combine(1)

    def arrive(i):
        cols = span_of(i)
        z_in("r", i)
        added = jnp.dot(
            home[...], zret[:, :, cols].reshape(128, span), preferred_element_type=F32
        )
        out_ref[:, cols] = (res[:, cols].astype(F32) + added).astype(BF16)

    phase("out0")
    arrive(0)
    phase("zon1r")
    z_on("r", 1, comb, zret, zretrel)
    phase("out1")
    arrive(1)
    phase("sent")
    ex.finish()
    phase()


def layer(
    q, k, v, w, res, gate, up, down, query_gain, key_gain, post_gain, pre_gain, ids, gw, fs
):
    hbm = pl.BlockSpec(memory_space=pl.ANY)
    vmem = pl.BlockSpec(memory_space=pltpu.VMEM)
    tokens, width = q.shape
    _, _, ff = gate.shape
    slots = pltpu.VMEM((4, 4, 2, 16, width), BF16)
    x_relay = pltpu.VMEM((2, 2, 2, 16, width), BF16)
    y_relay = pltpu.VMEM((2, 4, 16, width), BF16)
    z_block = pltpu.VMEM((4, 32, width), BF16)
    z_relay = pltpu.VMEM((2, 16, width), BF16)
    rows = pltpu.VMEM((tokens, width), BF16)
    return pl.pallas_call(
        layer_kernel,
        out_shape=jax.ShapeDtypeStruct((tokens, width), BF16),
        in_specs=[hbm] * 8 + [vmem] * 8,
        out_specs=vmem,
        scratch_shapes=[
            pltpu.VMEM((2, 4, 4, 128, 512), BF16),
            pltpu.VMEM((4, 512, 128), BF16),
            rows,
            pltpu.VMEM((tokens, 512), BF16),
            pltpu.VMEM((tokens, 512), BF16),
            pltpu.VMEM((width, width), BF16),
            rows,
            pltpu.VMEM((4, 1, 512), F32),
            pltpu.VMEM((4, 1, 512), F32),
            pltpu.VMEM((4, 128, 512), F32),
            rows,
            rows,
            rows,
            pltpu.VMEM((width, ff), BF16),
            pltpu.VMEM((width, ff), BF16),
            pltpu.VMEM((ff, width), BF16),
            pltpu.VMEM((4, 8, 128), F32),
            z_block, z_block, z_relay,
            slots, slots, x_relay, slots, y_relay,
            pltpu.VMEM((512, ff), F32),
            pltpu.VMEM((512, ff), F32),
            pltpu.VMEM((512, ff), BF16),
            slots, slots, y_relay, slots, x_relay,
            z_block, z_block, z_relay,
            pltpu.VMEM((512, 128), BF16),
            pltpu.VMEM((128, 512), BF16),
            pltpu.VMEM((128, 512), BF16),
            pltpu.VMEM((128, 128), BF16),
            pltpu.SemaphoreType.DMA((8,)),
            pltpu.SemaphoreType.DMA((COPIES,)),
            pltpu.SemaphoreType.DMA((COPIES,)),
        ],
        compiler_params=pltpu.CompilerParams(
            collective_id=0, has_side_effects=True, vmem_limit_bytes=62 * 1024 * 1024
        ),
        name="layer",
    )(
        q, k, v, w, res, gate, up, down, jnp.asarray(angle_tables()), query_gain.reshape(1, -1),
        key_gain.reshape(1, -1), post_gain.reshape(1, -1), pre_gain.reshape(1, -1), ids, gw, fs,
    )


def local(
    residual_in,
    query_proj,
    key_proj,
    value_proj,
    query_gain,
    key_gain,
    out_weight,
    post_gain,
    pre_gain,
    route_ids,
    group_weight,
    first_share,
    gate_weight,
    up_weight,
    down_weight,
):
    out = layer(
        query_proj[0], key_proj[0], value_proj[0], out_weight, residual_in[0],
        gate_weight, up_weight, down_weight, query_gain, key_gain, post_gain, pre_gain,
        route_ids[0].T, group_weight, first_share,
    )
    return out[None]


def solution(mesh):
    placed = (
        P("dp", "sp", None),
        P("dp", "sp", None),
        P("dp", "sp", None),
        P("dp", "sp", None),
        P(),
        P(),
        P(),
        P(),
        P(),
        P("dp", "sp", None),
        P("dp", "sp"),
        P("dp", "sp"),
        P(("sp", "dp"), None, None),
        P(("sp", "dp"), None, None),
        P(("sp", "dp"), None, None),
    )
    return jax.shard_map(
        local, mesh=mesh, in_specs=placed, out_specs=P("dp", "sp", None), check_vma=False
    )
```

time: 174 us -> 122 us (0.70)
  Pallas kernels: 51.2 us -> 119 us
  blocking collectives: 40.8 us -> 0 us
  waiting for transfers between devices: 29.7 us -> 0 us
  local copies, waits for them, and re-layouts: 28 us -> 1.88 us
  matrix products: 10.9 us -> 0 us
  other arithmetic: 6.92 us -> 0 us
  starting transfers between devices: 5.94 us -> 0 us
    pallas_call x1, Pallas kernels: 51.2 us -> 119 us  [layer(): pl.pallas_call(layer_kernel, out_shape=jax.ShapeDtypeStruct((tokens, widt...]
    all_to_all x1 -> x0, blocking collectives: 40.8 us -> none  [local(): lax.all_to_all(shaped, ('sp', 'dp'), split_axis=0, concat_axis=0, tiled=T...]
    all_to_all x1 -> x0, waiting for transfers between devices: 29.7 us -> none  [local(): lax.all_to_all(answered, ('sp', 'dp'), split_axis=0, concat_axis=0, tiled...]
    dot_general x2 -> x0, matrix products: 10.9 us -> none  [the longest x1 7.52 us: expert_ffn(): jnp.einsum('nesf,efd->nesd', hidden, down_weight, preferred_element_type=...]
    reshape x2 -> x0, local copies, waits for them, and re-layouts: 8.08 us -> none  [the longest x1 4.12 us: local(): outgoing.reshape(sp_count * dp_count, local_experts, capacity, model_width)]
    gather x2 -> x0, local copies, waits for them, and re-layouts: 7.57 us -> none  [the longest x1 4.22 us: local(): returned.reshape(expert_count * capacity, model_width)[slot_index]]
    convert_element_type x2 -> x0, local copies, waits for them, and re-layouts: 6.87 us -> none  [the longest x1 4.5 us: expert_ffn(): return jnp.einsum('nesf,efd->nesd', hidden, down_weight, preferred_elemen...]
    all_to_all x1 -> x0, starting transfers between devices: 5.94 us -> none  [local(): lax.all_to_all(answered, ('sp', 'dp'), split_axis=0, concat_axis=0, tiled...]
  transfers between devices with their start and end apart: 1 -> 0, of which waited for: 1 -> 0; matrix products, arithmetic and copies ran while one was open for 0% -> 0% of each run, Pallas kernels for 0% -> 0%
where the time goes in v3:
time: 122 us; the launch traced here: 121 us
  Pallas kernels  119 us (98%)
  local copies, waits for them, and re-layouts  1.88 us (2%)
    pallas_call x1, Pallas kernels, layer(): pl.pallas_call(layer_kernel, out_shape=jax.ShapeDtypeStruct((tokens, widt...  119 us

profile of v3, /device:TPU:1, one launch (start us, length us, event | category | flops | bytes accessed | tf_op | source)
XLA Modules:
  0.0 120.9 jit_solution(3458378797893166152)
XLA Ops:
  0.0 119.0 %layer.1 = bf16[128,2048]{1,0:T(8,128)(2,1)} custom-call(bf16[128,2048]{1,0:T(8,128)(2,1)} %bitcast.13, bf16[128,512]{1,0:T(8,128)(2,1)} %bitcast.15, bf16[128,512]{1,0:T(8,128)(2,1)} %bitcast.16, bf16[2048,2048]{1,0:T(8,128)(2,1)} %w_hbm.1, bf16[128,2048]{1,0:T(8,128)(2,1)} %bitcast.14, bf16[1,2048,512]{2,1,0:T(8,128)(2,1)} %gate_hbm.1, ...), custom_call_target="tpu_custom_call" | custom-call | tf_op jit(solution)/shard_map/layer/pallas_call | solution.py:677
  119.0 1.9 %copy.18 = bf16[1,128,2048]{2,1,0:T(8,128)(2,1)} copy(bf16[1,128,2048]{2,1,0:T(8,128)(2,1)} %bitcast.12) | data formatting | bytes 1048576

commit v4 on v3

--- a/solution.py
+++ b/solution.py
@@ -69,6 +69,7 @@
 class Exchange:
     def __init__(self, send_sem, recv_sem):
         self.send_sem, self.recv_sem, self.copies = send_sem, recv_sem, {}
+        self.unsent = []
 
     def start(self, name, src, dst, peer):
         i = len(self.copies)
@@ -82,19 +83,22 @@
         )
         assert name not in self.copies
         self.copies[name] = copy
+        self.unsent.append(copy)
         copy.start()
 
     def arrived(self, *names):
         for name in names:
             self.copies[name].wait_recv()
 
-    def finish(self):
-        for copy in self.copies.values():
+    def settle(self, count):
+        done = len(self.copies) - len(self.unsent)
+        for copy in self.unsent[: count - done]:
             copy.wait_send()
+        self.unsent = self.unsent[count - done :]
 
 
 ROUNDS = 2
-COPIES = 40 + 3 + ROUNDS * (2 * 84 + 2 * 6)
+COPIES = 40 + 3 + ROUNDS * 2 * (62 + 3)
 
 
 def iota(shape, dim):
@@ -107,8 +111,7 @@
     out_ref,
     kv, qt, q_raw, k_raw, v_raw, w, res, top, total, acc, att, mixed, normed,
     gate, up, down, meta,
-    zs, rows, zrel, xs, xr, xrel, yr, yrel, gates, lifts, hidden,
-    made, back, backrel, ret, retrel, comb, zret, zretrel,
+    zs, rows, xs, xr, yr, gates, lifts, hidden, made, back, ret, comb, zret,
     spread, pick1, pick2, home,
     local_sem, send_sem, recv_sem,
 ):
@@ -127,15 +130,13 @@
         loads[name] = pltpu.make_async_copy(src, dst, local_sem.at[i])
         loads[name].start()
 
-    ring = {
-        "z": (at(z + 1, x, y, c), at(z - 1, x, y, c)),
-        "x": (at(z, x + 1, y, c), at(z, x - 1, y, c)),
-        "y": (at(z, x, y + 1, c), at(z, x, y - 1, c)),
-        "yc": (at(z, x, y + 1, 1 - c), at(z, x, y - 1, 1 - c)),
-    }
-    across, twin = at(z + 2, x, y, c), at(z, x, y, 1 - c)
+    to_z = {s: at(z + s, x, y, c) for s in (1, 2, 3)}
+    to_x = {s: at(z, x + s, y, c) for s in (1, 2, 3)}
+    to_y = {(s, o): at(z, x, y + s, c if o == 0 else 1 - c) for s in range(4) for o in (0, 1)}
+    del to_y[0, 0]
+    ring = {"z": (to_z[1], to_z[3]), "x": (to_x[1], to_x[3])}
     barrier = pltpu.get_barrier_semaphore()
-    peers = [p for pair in ring.values() for p in pair] + [across, twin]
+    peers = [*to_z.values(), *to_x.values(), *to_y.values()]
     for peer in peers:
         pl.semaphore_signal(barrier, inc=1, device_id=peer, device_id_type=MESH)
     ex = Exchange(send_sem, recv_sem)
@@ -201,7 +202,7 @@
         both(p, "far", 0)
     ex.start("meta+", meta.at[0], meta.at[3], ring["z"][0])
     ex.start("meta-", meta.at[0], meta.at[1], ring["z"][1])
-    ex.start("meta2", meta.at[0], meta.at[2], across)
+    ex.start("meta2", meta.at[0], meta.at[2], to_z[2])
 
     phase("qturn")
     loads["q"].wait()
@@ -285,13 +286,15 @@
 
     scale = float(np.log2(np.e) / np.sqrt(HEAD_DIM))
 
-    def attend(r, opening):
+    def attend(blocks, opening=False):
         def one(g, carry):
             p, h = g // 2, g % 2
-            keys = kv[p, r, :, :, pl.ds(pl.multiple_of(h * 128, 128), 128)].reshape(512, 128)
-            values = kv[p, r, :, :, pl.ds(pl.multiple_of(256 + h * 128, 128), 128)].reshape(
-                512, 128
-            )
+
+            def part(offset):
+                cols = pl.ds(pl.multiple_of(offset + h * 128, 128), 128)
+                return jnp.concatenate([kv[p, a, b, :, cols] for a, b in blocks], axis=0)
+
+            keys, values = part(0), part(256)
             scores = lax.dot_general(
                 keys, qt[g], (((1,), (1,)), ((), ())), preferred_element_type=F32
             )
@@ -314,29 +317,37 @@
             acc[g] = out
             return carry
 
-        lax.fori_loop(0, KV_HEADS, one, 0)
+        lax.fori_loop(0, KV_HEADS, one, 0, unroll=2)
 
     phase("att0")
-    attend(0, True)
-    phase("far31")
-    for r in (3, 1):
+    attend([(0, 0), (0, 1), (0, 2), (0, 3)], opening=True)
+
+    def step_on(r, kind):
         for p in range(2):
-            got(p, "far", r)
-            both(p, "last", r)
+            got(p, kind, r)
+            if kind == "far":
+                both(p, "last", r)
+
+    phase("far3")
+    step_on(3, "far")
+    phase("att1")
+    attend([(3, 0), (3, 3), (1, 0), (1, 3)])
+    phase("far1")
+    step_on(1, "far")
     phase("far2")
-    for p in range(2):
-        got(p, "far", 2)
-        both(p, "last", 2)
+    step_on(2, "far")
+    phase("att2")
+    attend([(3, 1), (1, 1), (3, 2), (1, 2)])
+    phase("last03")
+    step_on(0, "last")
+    step_on(3, "last")
     phase("att3")
-    attend(3, False)
-    phase("att1")
-    attend(1, False)
-    phase("last")
-    for r in (0, 3, 1, 2):
-        for p in range(2):
-            got(p, "last", r)
-    phase("att2")
-    attend(2, False)
+    attend([(2, 0), (2, 3)])
+    phase("last12")
+    step_on(1, "last")
+    step_on(2, "last")
+    phase("att4")
+    attend([(2, 1), (2, 2)])
 
     phase("div")
     for g in range(KV_HEADS):
@@ -355,7 +366,7 @@
         mixed[:, cols] = jnp.dot(att[...], w[:, cols], preferred_element_type=F32).astype(BF16)
         return carry
 
-    lax.fori_loop(0, 4, project, 0)
+    lax.fori_loop(0, 4, project, 0, unroll=2)
     phase("norm")
 
     def norm(n, carry):
@@ -377,153 +388,69 @@
     def span_of(i):
         return pl.ds(i * span, span)
 
-    def z_parts(tag, i, src, dst, relay):
+    def z_out(tag, i, src, dst):
         cols = span_of(i)
-        top_rows, low_rows = pl.ds(0, 16), pl.ds(16, 16)
-        relays = relay.at[0, :, cols], relay.at[1, :, cols]
-        opposite = src.at[2, top_rows, cols], src.at[2, low_rows, cols]
-        finals = dst.at[2, top_rows, cols], dst.at[2, low_rows, cols]
-        return cols, relays, opposite, finals
-
-    def z_out(tag, i, src, dst, relay):
-        cols, relays, opposite, _ = z_parts(tag, i, src, dst, relay)
-        ex.start((tag, "z", "out+", i), opposite[0], relays[0], ring["z"][0])
-        ex.start((tag, "z", "out-", i), opposite[1], relays[1], ring["z"][1])
-
-    def z_direct(tag, i, src, dst):
-        cols = span_of(i)
-        ex.start((tag, "z", "+", i), src.at[1, :, cols], dst.at[3, :, cols], ring["z"][0])
-        ex.start((tag, "z", "-", i), src.at[3, :, cols], dst.at[1, :, cols], ring["z"][1])
-
-    def z_on(tag, i, src, dst, relay):
-        _, relays, _, finals = z_parts(tag, i, src, dst, relay)
-        for sign, relayed, final, to in zip("+-", relays, finals, ring["z"]):
-            ex.arrived((tag, "z", "out" + sign, i))
-            ex.start((tag, "z", "on" + sign, i), relayed, final, to)
+        for r in (2, 1, 3):
+            ex.start((tag, "z", r, i), src.at[r, :, cols], dst.at[4 - r, :, cols], to_z[r])
 
     def z_in(tag, i):
-        ex.arrived(*[(tag, "z", kind, i) for kind in ("+", "-", "on+", "on-")])
-
-    def swap(tag, i, src, mid, dst, x_relay, y_relay):
+        ex.arrived(*[(tag, "z", r, i) for r in (2, 1, 3)])
+
+    def swap(tag, i, src, mid, dst):
         a, b = pl.ds(i * span, step), pl.ds(i * span + step, step)
 
-        def block(ref, r, cols):
-            return lambda ry, rc: ref.at[r, ry, rc, :, cols]
-
-        def x_relays(cols):
-            return x_relay.at[0, :, :, :, cols], x_relay.at[1, :, :, :, cols]
-
-        def x_split(ref, cols):
-            return ref.at[2, pl.ds(0, 2), :, :, cols], ref.at[2, pl.ds(2, 2), :, :, cols]
-
-        def x_out(w, ref, cols):
-            for sign, part, relayed, to in zip("+-", x_split(ref, cols), x_relays(cols), ring["x"]):
-                ex.start((tag, w, "x", "out" + sign, i), part, relayed, to)
-
-        def x_plus(w, ref, to, cols):
+        def x_out(w, r, ref, to_ref, cols):
             ex.start(
-                (tag, w, "x", "+", i), ref.at[1, :, :, :, cols], to.at[3, :, :, :, cols],
-                ring["x"][0],
+                (tag, w, "x", r, i), ref.at[r, :, :, :, cols], to_ref.at[4 - r, :, :, :, cols],
+                to_x[r],
             )
 
-        def x_minus(w, ref, to, cols):
-            ex.start(
-                (tag, w, "x", "-", i), ref.at[3, :, :, :, cols], to.at[1, :, :, :, cols],
-                ring["x"][1],
-            )
-
-        def x_on(w, to_ref, cols):
-            finals = x_split(to_ref, cols)
-            for sign, relayed, final, to in zip("+-", x_relays(cols), finals, ring["x"]):
-                ex.arrived((tag, w, "x", "out" + sign, i))
-                ex.start((tag, w, "x", "on" + sign, i), relayed, final, to)
-
-        def y_names(w, r, kinds):
-            return [(tag, w, "y", r, kind, i) for kind in kinds]
-
-        def y_relays(r, cols):
-            return y_relay.at[0, r, :, cols], y_relay.at[1, r, :, cols]
-
-        def y_out(w, r, ref, cols):
-            part = block(ref, r, cols)
-            names = y_names(w, r, ("out+", "out-"))
-            for rc, relayed in enumerate(y_relays(r, cols)):
-                ex.start(names[rc], part(2, rc), relayed, ring["y"][rc])
-
-        def y_direct(w, r, ref, to_ref, cols):
-            part, final = block(ref, r, cols), block(to_ref, r, cols)
-            names = y_names(w, r, ("+", "-", "c+", "c-", "twin"))
-            ex.start(names[0], part(1, 0), final(3, 0), ring["y"][0])
-            ex.start(names[1], part(3, 0), final(1, 0), ring["y"][1])
-            ex.start(names[2], part(1, 1), final(3, 1), ring["yc"][0])
-            ex.start(names[3], part(3, 1), final(1, 1), ring["yc"][1])
-            ex.start(names[4], part(0, 1), final(0, 1), twin)
+        def x_in(w, r):
+            ex.arrived((tag, w, "x", 4 - r, i))
+
+        sides = [(2, 0), (2, 1), (1, 0), (3, 0), (1, 1), (3, 1), (0, 1)]
+
+        def y_out(w, r, ref, to_ref, cols):
+            for ry, rc in sides:
+                ex.start(
+                    (tag, w, "y", r, ry, rc, i), ref.at[r, ry, rc, :, cols],
+                    to_ref.at[r, (4 - ry) % 4, rc, :, cols], to_y[ry, rc],
+                )
             to_ref[r, 0, 0, :, cols] = ref[r, 0, 0, :, cols]
 
-        def y_on(w, r, to_ref, cols):
-            final = block(to_ref, r, cols)
-            outs, ons = y_names(w, r, ("out+", "out-")), y_names(w, r, ("on+", "on-"))
-            ex.arrived(outs[0])
-            ex.start(ons[0], y_relays(r, cols)[0], final(2, 0), ring["y"][0])
-            ex.arrived(outs[1])
-            ex.start(ons[1], y_relays(r, cols)[1], final(2, 1), ring["yc"][1])
-
         def y_in(w, r):
-            ex.arrived(*y_names(w, r, ("+", "-", "c+", "c-", "twin", "on+", "on-")))
-
-        def landing(r):
-            return dst if r == 0 else mid
-
-        def origin(r):
-            return src if r == 0 else mid
-
-        x_out("a", src, a)
-        y_out("b", 2, src, b)
-        y_out("b", 3, src, b)
-        y_out("b", 1, src, b)
-        x_plus("a", src, mid, a)
-        x_minus("a", src, mid, a)
-        y_direct("b", 2, src, mid, b)
-        y_direct("b", 3, src, mid, b)
-        y_direct("b", 1, src, mid, b)
-        y_out("a", 0, src, a)
-        y_out("b", 0, src, b)
+            ex.arrived(*[(tag, w, "y", r, ry, rc, i) for ry, rc in sides])
+
+        for r in (2, 1, 3):
+            x_out("a", r, src, mid, a)
+        for r in (2, 3, 1):
+            y_out("b", r, src, mid, b)
+        y_out("a", 0, src, dst, a)
+        y_out("b", 0, src, dst, b)
         yield
-        y_on("b", 2, mid, b)
-        y_on("b", 3, mid, b)
-        y_on("b", 1, mid, b)
-        y_direct("a", 0, src, dst, a)
-        y_direct("b", 0, src, dst, b)
-        x_on("a", mid, a)
+        y_in("b", 2)
+        x_out("b", 2, mid, dst, b)
+        y_in("b", 3)
+        x_out("b", 3, mid, dst, b)
+        x_in("a", 2)
+        y_out("a", 2, mid, dst, a)
+        y_in("b", 1)
+        x_out("b", 1, mid, dst, b)
+        x_in("a", 3)
+        y_out("a", 3, mid, dst, a)
+        x_in("a", 1)
+        y_out("a", 1, mid, dst, a)
         yield
-        y_on("a", 0, dst, a)
-        y_on("b", 0, dst, b)
-        y_in("b", 2)
-        x_out("b", mid, b)
-        ex.arrived((tag, "a", "x", "+", i))
-        y_out("a", 3, mid, a)
-        y_direct("a", 3, mid, dst, a)
-        ex.arrived((tag, "a", "x", "-", i))
-        y_out("a", 1, mid, a)
-        y_direct("a", 1, mid, dst, a)
-        y_in("b", 3)
-        x_minus("b", mid, dst, b)
-        y_in("b", 1)
-        x_plus("b", mid, dst, b)
+        y_in("a", 0)
+        y_in("b", 0)
+        y_in("a", 2)
+        x_in("b", 2)
         yield
-        ex.arrived((tag, "a", "x", "on+", i), (tag, "a", "x", "on-", i))
-        y_out("a", 2, mid, a)
-        y_direct("a", 2, mid, dst, a)
-        y_on("a", 3, dst, a)
-        y_on("a", 1, dst, a)
-        x_on("b", dst, b)
+        y_in("a", 3)
+        x_in("b", 3)
         yield
-        y_on("a", 2, dst, a)
-        yield
-        for r in range(4):
-            y_in("a", r)
-        y_in("b", 0)
-        ex.arrived(*[(tag, "b", "x", kind, i) for kind in ("+", "-", "on+", "on-")])
+        y_in("a", 1)
+        x_in("b", 1)
 
     def run(steps, count):
         for _ in range(count):
@@ -535,9 +462,7 @@
         packed = jnp.dot(pack, normed[:, cols], preferred_element_type=F32).astype(BF16)
         zs[:, :, cols] = packed.reshape(4, 32, span)
         rows[0, :, cols] = packed[0:32]
-        z_out("d", i, zs, rows, zrel)
-        if i == 0:
-            z_direct("d", 0, zs, rows)
+        z_out("d", i, zs, rows)
 
     def slots(i):
         cols = span_of(i)
@@ -548,12 +473,12 @@
         )
         xs[:, :, :, :, cols] = spaced.astype(BF16).reshape(4, 4, 2, 16, span)
 
-    def lift(i):
-        cols = span_of(i)
-        arrived = yr[:, :, :, :, cols].reshape(512, span)
+    def lift(i, at_r, count):
+        cols, at_rows = span_of(i), pl.ds(at_r * 128, count * 128)
+        arrived = yr[at_r : at_r + count, :, :, :, cols].reshape(count * 128, span)
         for sums, weight in ((gates, gate), (lifts, up)):
             product = jnp.dot(arrived, weight[cols, :], preferred_element_type=F32)
-            sums[...] = product if i == 0 else sums[...] + product
+            sums[at_rows, :] = product if i == 0 else sums[at_rows, :] + product
 
     def lower(i):
         cols = span_of(i)
@@ -568,79 +493,70 @@
         summed = (weight1 * one + weight2 * two).astype(BF16)
         comb[:, :, cols] = summed.reshape(4, 32, span)
         zret[0, :, cols] = summed[0:32]
-        z_out("r", i, comb, zret, zretrel)
-        z_direct("r", i, comb, zret)
-
-    there = [swap("d", i, xs, xr, yr, xrel, yrel) for i in range(ROUNDS)]
-    phase("zon0")
-    z_on("d", 0, zs, rows, zrel)
-    z_direct("d", 1, zs, rows)
+        z_out("r", i, comb, zret)
+
+    there = [swap("d", i, xs, xr, yr) for i in range(ROUNDS)]
     phase("zin0")
     slots(0)
-    phase("d0_start")
+    phase("d_start0")
     run(there[0], 1)
-    phase("d0_b")
-    run(there[0], 1)
-    phase("zon1")
-    z_on("d", 1, zs, rows, zrel)
-    phase("d0_c")
-    run(there[0], 1)
-    phase("zin1")
-    slots(1)
-    phase("d0_d")
-    run(there[0], 1)
-    phase("d1_start")
-    run(there[1], 1)
-    phase("d0_e")
-    run(there[0], 1)
-    phase("d1_b")
-    run(there[1], 1)
-    phase("d0_in")
-    run(there[0], 1)
-    phase("lift0")
+    ex.settle(43)
     loads["gate"].wait()
     loads["up"].wait()
-    lift(0)
-    for n in "cdef":
-        phase("d1_" + n)
-        run(there[1], 1)
-    phase("lift1")
-    lift(1)
+    for i in range(ROUNDS):
+        if i + 1 < ROUNDS:
+            phase("zin%d" % (i + 1))
+            slots(i + 1)
+        phase("d_mid%d" % i)
+        run(there[i], 1)
+        if i + 1 < ROUNDS:
+            phase("d_start%d" % (i + 1))
+            run(there[i + 1], 1)
+            phase("d_in%d" % i)
+            run(there[i], 3)
+            phase("lift%d" % i)
+            lift(i, 0, 4)
+            continue
+        ex.settle(43 + 3 * ROUNDS + 62 * i)
+        phase("d_in%d" % i)
+        run(there[i], 1)
+        phase("lift%d" % i)
+        lift(i, 0, 1)
+        lift(i, 2, 1)
+        phase("d_in%d" % i)
+        run(there[i], 1)
+        phase("lift%d" % i)
+        lift(i, 3, 1)
+        phase("d_in%d" % i)
+        run(there[i], 1)
+        phase("lift%d" % i)
+        lift(i, 1, 1)
     phase("silu")
     g = gates[...]
     hidden[...] = (g / (1.0 + jnp.exp(-g)) * lifts[...]).astype(BF16)
     loads["down"].wait()
 
-    home_way = [swap("r", i, made, back, ret, retrel, backrel) for i in range(ROUNDS)]
+    home_way = [swap("r", i, made, back, ret) for i in range(ROUNDS)]
     phase("lower0")
     lower(0)
-    phase("r0_start")
+    phase("r_start0")
     run(home_way[0], 1)
-    phase("lower1")
-    lower(1)
-    for n in "bcd":
-        phase("r0_" + n)
-        run(home_way[0], 1)
-    phase("r1_start")
-    run(home_way[1], 1)
-    phase("r0_e")
-    run(home_way[0], 1)
-    phase("r1_b")
-    run(home_way[1], 1)
-    phase("r0_in")
-    run(home_way[0], 1)
-    phase("combine0")
-    combine(0)
-    for n in "cd":
-        phase("r1_" + n)
-        run(home_way[1], 1)
-    phase("zon0r")
-    z_on("r", 0, comb, zret, zretrel)
-    for n in "ef":
-        phase("r1_" + n)
-        run(home_way[1], 1)
-    phase("combine1")
-    combine(1)
+    for i in range(ROUNDS):
+        if i + 1 < ROUNDS:
+            phase("lower%d" % (i + 1))
+            lower(i + 1)
+        phase("r_mid%d" % i)
+        run(home_way[i], 1)
+        if i + 1 < ROUNDS:
+            phase("r_start%d" % (i + 1))
+            run(home_way[i + 1], 1)
+        ex.settle(43 + 3 * ROUNDS + 62 * ROUNDS)
+        phase("r_in%d" % i)
+        run(home_way[i], 3)
+        if i + 1 == ROUNDS:
+            ex.settle(len(ex.copies) - 31)
+        phase("combine%d" % i)
+        combine(i)
 
     def arrive(i):
         cols = span_of(i)
@@ -650,14 +566,11 @@
         )
         out_ref[:, cols] = (res[:, cols].astype(F32) + added).astype(BF16)
 
-    phase("out0")
-    arrive(0)
-    phase("zon1r")
-    z_on("r", 1, comb, zret, zretrel)
-    phase("out1")
-    arrive(1)
+    for i in range(ROUNDS):
+        phase("out%d" % i)
+        arrive(i)
     phase("sent")
-    ex.finish()
+    ex.settle(COPIES)
     phase()
 
 
@@ -669,10 +582,7 @@
     tokens, width = q.shape
     _, _, ff = gate.shape
     slots = pltpu.VMEM((4, 4, 2, 16, width), BF16)
-    x_relay = pltpu.VMEM((2, 2, 2, 16, width), BF16)
-    y_relay = pltpu.VMEM((2, 4, 16, width), BF16)
     z_block = pltpu.VMEM((4, 32, width), BF16)
-    z_relay = pltpu.VMEM((2, 16, width), BF16)
     rows = pltpu.VMEM((tokens, width), BF16)
     return pl.pallas_call(
         layer_kernel,
@@ -697,13 +607,11 @@
             pltpu.VMEM((width, ff), BF16),
             pltpu.VMEM((ff, width), BF16),
             pltpu.VMEM((4, 8, 128), F32),
-            z_block, z_block, z_relay,
-            slots, slots, x_relay, slots, y_relay,
+            z_block, z_block, slots, slots, slots,
             pltpu.VMEM((512, ff), F32),
             pltpu.VMEM((512, ff), F32),
             pltpu.VMEM((512, ff), BF16),
-            slots, slots, y_relay, slots, x_relay,
-            z_block, z_block, z_relay,
+            slots, slots, slots, z_block, z_block,
             pltpu.VMEM((512, 128), BF16),
             pltpu.VMEM((128, 512), BF16),
             pltpu.VMEM((128, 512), BF16),

time: 122 us -> 109 us (0.89)
  Pallas kernels: 119 us -> 107 us
    pallas_call x1, Pallas kernels: 119 us -> 107 us  [layer(): pl.pallas_call(layer_kernel, out_shape=jax.ShapeDtypeStruct((tokens, widt...]
where the time goes in v4:
time: 109 us
  Pallas kernels  107 us (98%)
  local copies, waits for them, and re-layouts  1.88 us (2%)
    pallas_call x1, Pallas kernels, layer(): pl.pallas_call(layer_kernel, out_shape=jax.ShapeDtypeStruct((tokens, widt...  107 us

profile of v4, /device:TPU:1, one launch (start us, length us, event | category | flops | bytes accessed | tf_op | source)
XLA Modules:
  0.0 108.6 jit_solution(7647261569678298396)
XLA Ops:
  0.0 106.7 %layer.1 = bf16[128,2048]{1,0:T(8,128)(2,1)} custom-call(bf16[128,2048]{1,0:T(8,128)(2,1)} %bitcast.13, bf16[128,512]{1,0:T(8,128)(2,1)} %bitcast.15, bf16[128,512]{1,0:T(8,128)(2,1)} %bitcast.16, bf16[2048,2048]{1,0:T(8,128)(2,1)} %w_hbm.1, bf16[128,2048]{1,0:T(8,128)(2,1)} %bitcast.14, bf16[1,2048,512]{2,1,0:T(8,128)(2,1)} %gate_hbm.1, ...), custom_call_target="tpu_custom_call" | custom-call | tf_op jit(solution)/shard_map/layer/pallas_call | solution.py:587
  106.7 1.9 %copy.18 = bf16[1,128,2048]{2,1,0:T(8,128)(2,1)} copy(bf16[1,128,2048]{2,1,0:T(8,128)(2,1)} %bitcast.12) | data formatting | bytes 1048576

commit v5 on v4

--- a/solution.py
+++ b/solution.py
@@ -97,7 +97,8 @@
         self.unsent = self.unsent[count - done :]
 
 
-ROUNDS = 2
+SPANS = {"d": (512, 1024, 512), "r": (1024, 512, 512)}
+ROUNDS = 3
 COPIES = 40 + 3 + ROUNDS * 2 * (62 + 3)
 
 
@@ -107,8 +108,9 @@
 
 def layer_kernel(
     q_hbm, k_hbm, v_hbm, w_hbm, res_hbm, gate_hbm, up_hbm, down_hbm,
+    table_hbm, qg_hbm, kg_hbm, postg_hbm, preg_hbm, ids_hbm, gw_hbm, fs_hbm,
+    out_ref,
     table_ref, qg_ref, kg_ref, postg_ref, preg_ref, ids_ref, gw_ref, fs_ref,
-    out_ref,
     kv, qt, q_raw, k_raw, v_raw, w, res, top, total, acc, att, mixed, normed,
     gate, up, down, meta,
     zs, rows, xs, xr, yr, gates, lifts, hidden, made, back, ret, comb, zret,
@@ -122,7 +124,10 @@
     loads = {}
     for i, (name, src, dst) in enumerate(
         [
-            ("k", k_hbm, k_raw), ("v", v_hbm, v_raw), ("q", q_hbm, q_raw), ("res", res_hbm, res),
+            ("table", table_hbm, table_ref), ("k", k_hbm, k_raw), ("kg", kg_hbm, kg_ref),
+            ("v", v_hbm, v_raw), ("ids", ids_hbm, ids_ref), ("gw", gw_hbm, gw_ref),
+            ("fs", fs_hbm, fs_ref), ("qg", qg_hbm, qg_ref), ("q", q_hbm, q_raw),
+            ("postg", postg_hbm, postg_ref), ("preg", preg_hbm, preg_ref), ("res", res_hbm, res),
             ("w", w_hbm, w), ("gate", gate_hbm.at[0], gate), ("up", up_hbm.at[0], up),
             ("down", down_hbm.at[0], down),
         ]
@@ -150,12 +155,16 @@
             halves.append(jnp.where(lane < 64, row, table_ref[which, 32 : 32 + GRID_W, :]))
         return jnp.concatenate(halves, axis=0)
 
+    loads["table"].wait()
     cos, sin = table(0), table(1)
+    for name in ("ids", "gw", "fs"):
+        loads[name].wait()
     meta[0, 0:2, :] = ids_ref[...].astype(F32)
     meta[0, 2:3, :] = gw_ref[...]
     meta[0, 3:4, :] = fs_ref[...]
     meta[0, 4:8, :] = jnp.zeros((4, 128), F32)
     loads["k"].wait()
+    loads["kg"].wait()
     for h in range(KV_HEADS):
         raw = k_raw[:, h * 128 : (h + 1) * 128].astype(F32)
         kv[h // 2, 0, 0, :, (h % 2) * 128 : (h % 2 + 1) * 128] = turn(raw, kg_ref[...], cos, sin)
@@ -206,6 +215,7 @@
 
     phase("qturn")
     loads["q"].wait()
+    loads["qg"].wait()
     for h in range(HEADS):
         raw = q_raw[:, h * 128 : (h + 1) * 128].astype(F32)
         qt[h // 4, (h % 4) * 128 : (h % 4 + 1) * 128, :] = turn(raw, qg_ref[...], cos, sin)
@@ -317,7 +327,7 @@
             acc[g] = out
             return carry
 
-        lax.fori_loop(0, KV_HEADS, one, 0, unroll=2)
+        lax.fori_loop(0, KV_HEADS, one, 0, unroll=len(blocks) < 4 or 2)
 
     phase("att0")
     attend([(0, 0), (0, 1), (0, 2), (0, 3)], opening=True)
@@ -345,9 +355,12 @@
     attend([(2, 0), (2, 3)])
     phase("last12")
     step_on(1, "last")
+    phase("att4")
+    attend([(2, 1)])
+    phase("last2")
     step_on(2, "last")
-    phase("att4")
-    attend([(2, 1), (2, 2)])
+    phase("att5")
+    attend([(2, 2)])
 
     phase("div")
     for g in range(KV_HEADS):
@@ -357,7 +370,8 @@
             att[:, head * 128 : (head + 1) * 128] = (
                 scaled[:, h * 128 : (h + 1) * 128].T.astype(BF16)
             )
-    loads["res"].wait()
+    for name in ("postg", "preg", "res"):
+        loads[name].wait()
     loads["w"].wait()
     phase("proj")
 
@@ -366,7 +380,7 @@
         mixed[:, cols] = jnp.dot(att[...], w[:, cols], preferred_element_type=F32).astype(BF16)
         return carry
 
-    lax.fori_loop(0, 4, project, 0, unroll=2)
+    lax.fori_loop(0, 4, project, 0, unroll=True)
     phase("norm")
 
     def norm(n, carry):
@@ -380,16 +394,16 @@
         normed[at_rows, :] = s.astype(BF16)
         return carry
 
-    lax.fori_loop(0, 4, norm, 0)
-
-    span = width // ROUNDS
-    step = span // 2
-
-    def span_of(i):
-        return pl.ds(i * span, span)
+    lax.fori_loop(0, 4, norm, 0, unroll=2)
+
+    def begin_of(tag, i):
+        return sum(SPANS[tag][:i])
+
+    def span_of(tag, i):
+        return pl.ds(begin_of(tag, i), SPANS[tag][i])
 
     def z_out(tag, i, src, dst):
-        cols = span_of(i)
+        cols = span_of(tag, i)
         for r in (2, 1, 3):
             ex.start((tag, "z", r, i), src.at[r, :, cols], dst.at[4 - r, :, cols], to_z[r])
 
@@ -397,7 +411,8 @@
         ex.arrived(*[(tag, "z", r, i) for r in (2, 1, 3)])
 
     def swap(tag, i, src, mid, dst):
-        a, b = pl.ds(i * span, step), pl.ds(i * span + step, step)
+        step = SPANS[tag][i] // 2
+        a, b = pl.ds(begin_of(tag, i), step), pl.ds(begin_of(tag, i) + step, step)
 
         def x_out(w, r, ref, to_ref, cols):
             ex.start(
@@ -423,6 +438,7 @@
 
         for r in (2, 1, 3):
             x_out("a", r, src, mid, a)
+        yield
         for r in (2, 3, 1):
             y_out("b", r, src, mid, b)
         y_out("a", 0, src, dst, a)
@@ -458,111 +474,116 @@
 
     phase("pack")
     for i in range(ROUNDS):
-        cols = span_of(i)
+        cols = span_of("d", i)
         packed = jnp.dot(pack, normed[:, cols], preferred_element_type=F32).astype(BF16)
-        zs[:, :, cols] = packed.reshape(4, 32, span)
+        zs[:, :, cols] = packed.reshape(4, 32, SPANS["d"][i])
         rows[0, :, cols] = packed[0:32]
         z_out("d", i, zs, rows)
 
     def slots(i):
-        cols = span_of(i)
+        cols = span_of("d", i)
         z_in("d", i)
         phase("slots%d" % i)
         spaced = jnp.dot(
-            spread[...], rows[:, :, cols].reshape(128, span), preferred_element_type=F32
+            spread[...], rows[:, :, cols].reshape(128, SPANS["d"][i]), preferred_element_type=F32
         )
-        xs[:, :, :, :, cols] = spaced.astype(BF16).reshape(4, 4, 2, 16, span)
+        xs[:, :, :, :, cols] = spaced.astype(BF16).reshape(4, 4, 2, 16, SPANS["d"][i])
 
     def lift(i, at_r, count):
-        cols, at_rows = span_of(i), pl.ds(at_r * 128, count * 128)
-        arrived = yr[at_r : at_r + count, :, :, :, cols].reshape(count * 128, span)
+        cols, at_rows = span_of("d", i), pl.ds(at_r * 128, count * 128)
+        arrived = yr[at_r : at_r + count, :, :, :, cols].reshape(count * 128, SPANS["d"][i])
         for sums, weight in ((gates, gate), (lifts, up)):
             product = jnp.dot(arrived, weight[cols, :], preferred_element_type=F32)
             sums[at_rows, :] = product if i == 0 else sums[at_rows, :] + product
 
-    def lower(i):
-        cols = span_of(i)
+    def lower(i, half):
+        step = SPANS["r"][i] // 2
+        cols = pl.ds(begin_of("r", i) + half * step, step)
         produced = jnp.dot(hidden[...], down[:, cols], preferred_element_type=F32)
-        made[:, :, :, :, cols] = produced.astype(BF16).reshape(4, 4, 2, 16, span)
+        made[:, :, :, :, cols] = produced.astype(BF16).reshape(4, 4, 2, 16, step)
 
     def combine(i):
-        cols = span_of(i)
-        returned = ret[:, :, :, :, cols].reshape(512, span)
+        cols = span_of("r", i)
+        returned = ret[:, :, :, :, cols].reshape(512, SPANS["r"][i])
         one = jnp.dot(pick1[...], returned, preferred_element_type=F32)
         two = jnp.dot(pick2[...], returned, preferred_element_type=F32)
         summed = (weight1 * one + weight2 * two).astype(BF16)
-        comb[:, :, cols] = summed.reshape(4, 32, span)
+        comb[:, :, cols] = summed.reshape(4, 32, SPANS["r"][i])
         zret[0, :, cols] = summed[0:32]
         z_out("r", i, comb, zret)
 
     there = [swap("d", i, xs, xr, yr) for i in range(ROUNDS)]
-    phase("zin0")
-    slots(0)
-    phase("d_start0")
-    run(there[0], 1)
+    def begin(i):
+        phase("zin%d" % i)
+        slots(i)
+        phase("d_start%d" % i)
+        run(there[i], 2)
+
+    def middle(i):
+        phase("d_mid%d" % i)
+        run(there[i], 1)
+
+    begin(0)
     ex.settle(43)
+    begin(1)
+    middle(0)
+    begin(2)
+    middle(1)
+    phase("d_in0")
+    run(there[0], 3)
+    phase("lift0")
     loads["gate"].wait()
     loads["up"].wait()
-    for i in range(ROUNDS):
-        if i + 1 < ROUNDS:
-            phase("zin%d" % (i + 1))
-            slots(i + 1)
-        phase("d_mid%d" % i)
-        run(there[i], 1)
-        if i + 1 < ROUNDS:
-            phase("d_start%d" % (i + 1))
-            run(there[i + 1], 1)
+    lift(0, 0, 4)
+    middle(2)
+    ex.settle(43 + 3 * ROUNDS + 62)
+    for i in (1, 2):
+        for pieces in (((0, 1), (2, 1)), ((3, 1),), ((1, 1),)):
             phase("d_in%d" % i)
-            run(there[i], 3)
+            run(there[i], 1)
             phase("lift%d" % i)
-            lift(i, 0, 4)
-            continue
-        ex.settle(43 + 3 * ROUNDS + 62 * i)
-        phase("d_in%d" % i)
-        run(there[i], 1)
-        phase("lift%d" % i)
-        lift(i, 0, 1)
-        lift(i, 2, 1)
-        phase("d_in%d" % i)
-        run(there[i], 1)
-        phase("lift%d" % i)
-        lift(i, 3, 1)
-        phase("d_in%d" % i)
-        run(there[i], 1)
-        phase("lift%d" % i)
-        lift(i, 1, 1)
+            for piece in pieces:
+                lift(i, *piece)
     phase("silu")
     g = gates[...]
     hidden[...] = (g / (1.0 + jnp.exp(-g)) * lifts[...]).astype(BF16)
     loads["down"].wait()
 
     home_way = [swap("r", i, made, back, ret) for i in range(ROUNDS)]
-    phase("lower0")
-    lower(0)
-    phase("r_start0")
-    run(home_way[0], 1)
-    for i in range(ROUNDS):
-        if i + 1 < ROUNDS:
-            phase("lower%d" % (i + 1))
-            lower(i + 1)
+    def begin(i):
+        for half in range(2):
+            phase("lower%d" % i)
+            lower(i, half)
+            phase("r_start%d" % i)
+            run(home_way[i], 1)
+
+    def middle(i):
         phase("r_mid%d" % i)
         run(home_way[i], 1)
-        if i + 1 < ROUNDS:
-            phase("r_start%d" % (i + 1))
-            run(home_way[i + 1], 1)
-        ex.settle(43 + 3 * ROUNDS + 62 * ROUNDS)
+
+    def end(i):
         phase("r_in%d" % i)
         run(home_way[i], 3)
-        if i + 1 == ROUNDS:
-            ex.settle(len(ex.copies) - 31)
         phase("combine%d" % i)
         combine(i)
 
+    begin(0)
+    begin(1)
+    middle(0)
+    begin(2)
+    middle(1)
+    ex.settle(43 + 3 * ROUNDS + 62 * ROUNDS)
+    end(0)
+    middle(2)
+    end(1)
+    ex.settle(len(ex.copies) - 40)
+    end(2)
+
     def arrive(i):
-        cols = span_of(i)
+        cols = span_of("r", i)
         z_in("r", i)
         added = jnp.dot(
-            home[...], zret[:, :, cols].reshape(128, span), preferred_element_type=F32
+            home[...], zret[:, :, cols].reshape(128, SPANS["r"][i]), preferred_element_type=F32
         )
         out_ref[:, cols] = (res[:, cols].astype(F32) + added).astype(BF16)
 
@@ -577,7 +598,7 @@
 def layer(
     q, k, v, w, res, gate, up, down, query_gain, key_gain, post_gain, pre_gain, ids, gw, fs
 ):
-    hbm = pl.BlockSpec(memory_space=pl.ANY)
+    hbm = pl.BlockSpec(memory_space=pltpu.HBM)
     vmem = pl.BlockSpec(memory_space=pltpu.VMEM)
     tokens, width = q.shape
     _, _, ff = gate.shape
@@ -586,10 +607,18 @@
     rows = pltpu.VMEM((tokens, width), BF16)
     return pl.pallas_call(
         layer_kernel,
-        out_shape=jax.ShapeDtypeStruct((tokens, width), BF16),
-        in_specs=[hbm] * 8 + [vmem] * 8,
+        out_shape=pltpu.VMEM((tokens, width), BF16),
+        in_specs=[hbm] * 16,
         out_specs=vmem,
         scratch_shapes=[
+            pltpu.VMEM((2, 32 + GRID_W, HEAD_DIM), F32),
+            pltpu.VMEM((1, HEAD_DIM), F32),
+            pltpu.VMEM((1, HEAD_DIM), F32),
+            pltpu.VMEM((1, width), F32),
+            pltpu.VMEM((1, width), F32),
+            pltpu.VMEM((2, tokens), jnp.int32),
+            pltpu.VMEM((1, tokens), F32),
+            pltpu.VMEM((1, tokens), F32),
             pltpu.VMEM((2, 4, 4, 128, 512), BF16),
             pltpu.VMEM((4, 512, 128), BF16),
             rows,
@@ -616,12 +645,12 @@
             pltpu.VMEM((128, 512), BF16),
             pltpu.VMEM((128, 512), BF16),
             pltpu.VMEM((128, 128), BF16),
-            pltpu.SemaphoreType.DMA((8,)),
+            pltpu.SemaphoreType.DMA((16,)),
             pltpu.SemaphoreType.DMA((COPIES,)),
             pltpu.SemaphoreType.DMA((COPIES,)),
         ],
         compiler_params=pltpu.CompilerParams(
-            collective_id=0, has_side_effects=True, vmem_limit_bytes=62 * 1024 * 1024
+            collective_id=0, has_side_effects=True, vmem_limit_bytes=60 * 1024 * 1024
         ),
         name="layer",
     )(

time: 109 us -> 103 us (0.945)
  Pallas kernels: 107 us -> 102 us
    pallas_call x1, Pallas kernels: 107 us -> 102 us  [layer(): pl.pallas_call(layer_kernel, out_shape=pltpu.VMEM((tokens, width), BF16),...]
where the time goes in v5:
time: 103 us; the launch traced here: 102 us
  Pallas kernels  102 us (99%)
    pallas_call x1, Pallas kernels, layer(): pl.pallas_call(layer_kernel, out_shape=pltpu.VMEM((tokens, width), BF16),...  102 us

profile of v5, /device:TPU:1, one launch (start us, length us, event | category | flops | bytes accessed | tf_op | source)
XLA Modules:
  0.0 102.4 jit_solution(13357959442406771786)
XLA Ops:
  0.0 101.6 %layer.1 = bf16[128,2048]{1,0:T(8,128)(2,1)S(1)} custom-call(bf16[128,2048]{1,0:T(8,128)(2,1)} %bitcast.13, bf16[128,512]{1,0:T(8,128)(2,1)} %bitcast.15, bf16[128,512]{1,0:T(8,128)(2,1)} %bitcast.16, bf16[2048,2048]{1,0:T(8,128)(2,1)} %w_hbm.1, bf16[128,2048]{1,0:T(8,128)(2,1)} %bitcast.14, bf16[1,2048,512]{2,1,0:T(8,128)(2,1)} %gate_hbm.1, ...), custom_call_target="tpu_custom_call" | custom-call | tf_op jit(solution)/shard_map/layer/pallas_call | solution.py:608
  101.7 0.8 copy.18

commit v6 on v5

--- a/solution.py
+++ b/solution.py
@@ -68,38 +68,30 @@
 
 class Exchange:
     def __init__(self, send_sem, recv_sem):
-        self.send_sem, self.recv_sem, self.copies = send_sem, recv_sem, {}
-        self.unsent = []
-
-    def start(self, name, src, dst, peer):
-        i = len(self.copies)
-        copy = pltpu.make_async_remote_copy(
+        self.send_sem, self.recv_sem = send_sem, recv_sem
+        self.sent_at, self.got_at = {}, {}
+
+    def start(self, sent, got, src, dst, peer):
+        pltpu.make_async_remote_copy(
             src_ref=src,
             dst_ref=dst,
-            send_sem=self.send_sem.at[i],
-            recv_sem=self.recv_sem.at[i],
+            send_sem=self.send_sem.at[self.sent_at.setdefault(sent, len(self.sent_at))],
+            recv_sem=self.recv_sem.at[self.got_at.setdefault(got, len(self.got_at))],
             device_id=peer,
             device_id_type=MESH,
-        )
-        assert name not in self.copies
-        self.copies[name] = copy
-        self.unsent.append(copy)
-        copy.start()
-
-    def arrived(self, *names):
-        for name in names:
-            self.copies[name].wait_recv()
-
-    def settle(self, count):
-        done = len(self.copies) - len(self.unsent)
-        for copy in self.unsent[: count - done]:
-            copy.wait_send()
-        self.unsent = self.unsent[count - done :]
-
-
-SPANS = {"d": (512, 1024, 512), "r": (1024, 512, 512)}
-ROUNDS = 3
-COPIES = 40 + 3 + ROUNDS * 2 * (62 + 3)
+        ).start()
+
+    def arrived(self, got, like):
+        pltpu.make_async_copy(like, like, self.recv_sem.at[self.got_at[got]]).wait()
+
+    def settle(self, sent, like):
+        pltpu.make_async_copy(like, like, self.send_sem.at[self.sent_at[sent]]).wait()
+
+
+SPANS = {"d": (256, 512, 768, 512), "r": (512, 768, 512, 256)}
+ROUNDS = 4
+SENT = 5 + 4 * ROUNDS
+GOT = 21 + 2 * 8 * ROUNDS
 
 
 def iota(shape, dim):
@@ -114,13 +106,22 @@
     kv, qt, q_raw, k_raw, v_raw, w, res, top, total, acc, att, mixed, normed,
     gate, up, down, meta,
     zs, rows, xs, xr, yr, gates, lifts, hidden, made, back, ret, comb, zret,
-    spread, pick1, pick2, home,
+    spread, pick1, pick2, home, tally,
     local_sem, send_sem, recv_sem,
 ):
     z, x, y, c = position()
     width = q_raw.shape[1]
     phase = Phase()
     phase("turn")
+    to_z = {s: at(z + s, x, y, c) for s in (1, 2, 3)}
+    to_x = {s: at(z, x + s, y, c) for s in (1, 2, 3)}
+    to_y = {(s, o): at(z, x, y + s, c if o == 0 else 1 - c) for s in range(4) for o in (0, 1)}
+    del to_y[0, 0]
+    ring = {"z": (to_z[1], to_z[3]), "x": (to_x[1], to_x[3])}
+    barrier = pltpu.get_barrier_semaphore()
+    peers = [*to_z.values(), *to_x.values(), *to_y.values()]
+    for peer in peers:
+        pl.semaphore_signal(barrier, inc=1, device_id=peer, device_id_type=MESH)
     loads = {}
     for i, (name, src, dst) in enumerate(
         [
@@ -134,16 +135,6 @@
     ):
         loads[name] = pltpu.make_async_copy(src, dst, local_sem.at[i])
         loads[name].start()
-
-    to_z = {s: at(z + s, x, y, c) for s in (1, 2, 3)}
-    to_x = {s: at(z, x + s, y, c) for s in (1, 2, 3)}
-    to_y = {(s, o): at(z, x, y + s, c if o == 0 else 1 - c) for s in range(4) for o in (0, 1)}
-    del to_y[0, 0]
-    ring = {"z": (to_z[1], to_z[3]), "x": (to_x[1], to_x[3])}
-    barrier = pltpu.get_barrier_semaphore()
-    peers = [*to_z.values(), *to_x.values(), *to_y.values()]
-    for peer in peers:
-        pl.semaphore_signal(barrier, inc=1, device_id=peer, device_id_type=MESH)
     ex = Exchange(send_sem, recv_sem)
 
     lane = iota((GRID_W, HEAD_DIM), 1)
@@ -180,7 +171,6 @@
     low, high = pl.ds(0, 64), pl.ds(64, 64)
 
     def both(p, kind, r=0):
-        names = ((kind, p, r, "+"), (kind, p, r, "-"))
         if kind == "own":
             peer = ring[first[p]]
             pairs = (kv.at[p, 0, 0], kv.at[p, 0, 3]), (kv.at[p, 0, 0], kv.at[p, 0, 1])
@@ -199,19 +189,19 @@
                 (kv.at[p, 3, r, low], kv.at[p, 2, r, low]),
                 (kv.at[p, 1, r, high], kv.at[p, 2, r, high]),
             )
-        for name, (src, dst), to in zip(names, pairs, peer):
-            ex.start(name, src, dst, to)
+        for (src, dst), to in zip(pairs, peer):
+            ex.start(kind, (kind, p, r), src, dst, to)
 
     def got(p, kind, r=0):
-        ex.arrived((kind, p, r, "+"), (kind, p, r, "-"))
+        whole = kind in ("own", "far")
+        ex.arrived((kind, p, r), kv.at[p, 0, pl.ds(0, 2 if whole else 1)])
 
     for p in range(2):
         both(p, "own")
     for p in range(2):
         both(p, "far", 0)
-    ex.start("meta+", meta.at[0], meta.at[3], ring["z"][0])
-    ex.start("meta-", meta.at[0], meta.at[1], ring["z"][1])
-    ex.start("meta2", meta.at[0], meta.at[2], to_z[2])
+    for r in (1, 2, 3):
+        ex.start("meta", "meta", meta.at[0], meta.at[4 - r], to_z[r])
 
     phase("qturn")
     loads["q"].wait()
@@ -257,7 +247,7 @@
         both(p, "last", 0)
 
     phase("tables2")
-    ex.arrived("meta+", "meta-", "meta2")
+    ex.arrived("meta", meta.at[pl.ds(0, 3)])
     stacks = [[], [], [], []]
     for r in range(4):
         inside = (meta[r, 0:1, :].astype(jnp.int32) >> 5) == z
@@ -402,13 +392,17 @@
     def span_of(tag, i):
         return pl.ds(begin_of(tag, i), SPANS[tag][i])
 
+    def like(count, columns):
+        return tally.at[pl.ds(0, count), pl.ds(0, columns)]
+
     def z_out(tag, i, src, dst):
         cols = span_of(tag, i)
         for r in (2, 1, 3):
-            ex.start((tag, "z", r, i), src.at[r, :, cols], dst.at[4 - r, :, cols], to_z[r])
+            name = (tag, "z", i)
+            ex.start(name, name, src.at[r, :, cols], dst.at[4 - r, :, cols], to_z[r])
 
     def z_in(tag, i):
-        ex.arrived(*[(tag, "z", r, i) for r in (2, 1, 3)])
+        ex.arrived((tag, "z", i), like(96, SPANS[tag][i]))
 
     def swap(tag, i, src, mid, dst):
         step = SPANS[tag][i] // 2
@@ -416,25 +410,26 @@
 
         def x_out(w, r, ref, to_ref, cols):
             ex.start(
-                (tag, w, "x", r, i), ref.at[r, :, :, :, cols], to_ref.at[4 - r, :, :, :, cols],
-                to_x[r],
+                (tag, i), (tag, "x", r, i) if w == "a" else (tag, i),
+                ref.at[r, :, :, :, cols], to_ref.at[4 - r, :, :, :, cols], to_x[r],
             )
 
-        def x_in(w, r):
-            ex.arrived((tag, w, "x", 4 - r, i))
+        def x_in(r):
+            ex.arrived((tag, "x", 4 - r, i), like(128, step))
 
         sides = [(2, 0), (2, 1), (1, 0), (3, 0), (1, 1), (3, 1), (0, 1)]
 
         def y_out(w, r, ref, to_ref, cols):
             for ry, rc in sides:
                 ex.start(
-                    (tag, w, "y", r, ry, rc, i), ref.at[r, ry, rc, :, cols],
-                    to_ref.at[r, (4 - ry) % 4, rc, :, cols], to_y[ry, rc],
+                    (tag, i), (tag, "y", r, i) if w == "b" and r else (tag, i),
+                    ref.at[r, ry, rc, :, cols], to_ref.at[r, (4 - ry) % 4, rc, :, cols],
+                    to_y[ry, rc],
                 )
             to_ref[r, 0, 0, :, cols] = ref[r, 0, 0, :, cols]
 
-        def y_in(w, r):
-            ex.arrived(*[(tag, w, "y", r, ry, rc, i) for ry, rc in sides])
+        def y_in(r):
+            ex.arrived((tag, "y", r, i), like(112, step))
 
         for r in (2, 1, 3):
             x_out("a", r, src, mid, a)
@@ -444,29 +439,25 @@
         y_out("a", 0, src, dst, a)
         y_out("b", 0, src, dst, b)
         yield
-        y_in("b", 2)
+        y_in(2)
         x_out("b", 2, mid, dst, b)
-        y_in("b", 3)
+        y_in(3)
         x_out("b", 3, mid, dst, b)
-        x_in("a", 2)
+        x_in(2)
         y_out("a", 2, mid, dst, a)
-        y_in("b", 1)
+        y_in(1)
         x_out("b", 1, mid, dst, b)
-        x_in("a", 3)
+        x_in(3)
         y_out("a", 3, mid, dst, a)
-        x_in("a", 1)
+        x_in(1)
         y_out("a", 1, mid, dst, a)
         yield
-        y_in("a", 0)
-        y_in("b", 0)
-        y_in("a", 2)
-        x_in("b", 2)
-        yield
-        y_in("a", 3)
-        x_in("b", 3)
-        yield
-        y_in("a", 1)
-        x_in("b", 1)
+        ex.arrived((tag, i), like(5 * 112 + 3 * 128, step))
+
+    def settle_swaps(tag):
+        for i in range(ROUNDS):
+            ex.settle((tag, "z", i), like(96, SPANS[tag][i]))
+            ex.settle((tag, i), like(4 * 112 + 3 * 128, SPANS[tag][i]))
 
     def run(steps, count):
         for _ in range(count):
@@ -523,30 +514,38 @@
         phase("d_mid%d" % i)
         run(there[i], 1)
 
+    def done(i):
+        phase("d_in%d" % i)
+        run(there[i], 1)
+        phase("lift%d" % i)
+        lift(i, 0, 4)
+
     begin(0)
-    ex.settle(43)
+    ex.settle("own", kv.at[0, 0])
+    ex.settle("relay", kv.at[0, 0, pl.ds(0, 2)])
+    ex.settle("far", kv.at[0])
+    ex.settle("last", kv.at[0, pl.ds(0, 2)])
+    ex.settle("meta", meta.at[pl.ds(0, 3)])
     begin(1)
     middle(0)
     begin(2)
     middle(1)
-    phase("d_in0")
-    run(there[0], 3)
-    phase("lift0")
     loads["gate"].wait()
     loads["up"].wait()
-    lift(0, 0, 4)
+    done(0)
+    begin(3)
     middle(2)
-    ex.settle(43 + 3 * ROUNDS + 62)
-    for i in (1, 2):
-        for pieces in (((0, 1), (2, 1)), ((3, 1),), ((1, 1),)):
-            phase("d_in%d" % i)
-            run(there[i], 1)
-            phase("lift%d" % i)
-            for piece in pieces:
-                lift(i, *piece)
-    phase("silu")
-    g = gates[...]
-    hidden[...] = (g / (1.0 + jnp.exp(-g)) * lifts[...]).astype(BF16)
+    done(1)
+    middle(3)
+    done(2)
+    phase("d_in3")
+    run(there[3], 1)
+    phase("lift3")
+    for half in range(2):
+        lift(3, 2 * half, 2)
+        at_rows = pl.ds(256 * half, 256)
+        g = gates[at_rows, :]
+        hidden[at_rows, :] = (g / (1.0 + jnp.exp(-g)) * lifts[at_rows, :]).astype(BF16)
     loads["down"].wait()
 
     home_way = [swap("r", i, made, back, ret) for i in range(ROUNDS)]
@@ -563,7 +562,7 @@
 
     def end(i):
         phase("r_in%d" % i)
-        run(home_way[i], 3)
+        run(home_way[i], 1)
         phase("combine%d" % i)
         combine(i)
 
@@ -572,12 +571,14 @@
     middle(0)
     begin(2)
     middle(1)
-    ex.settle(43 + 3 * ROUNDS + 62 * ROUNDS)
+    settle_swaps("d")
     end(0)
+    begin(3)
     middle(2)
     end(1)
-    ex.settle(len(ex.copies) - 40)
+    middle(3)
     end(2)
+    end(3)
 
     def arrive(i):
         cols = span_of("r", i)
@@ -591,7 +592,7 @@
         phase("out%d" % i)
         arrive(i)
     phase("sent")
-    ex.settle(COPIES)
+    settle_swaps("r")
     phase()
 
 
@@ -645,9 +646,10 @@
             pltpu.VMEM((128, 512), BF16),
             pltpu.VMEM((128, 512), BF16),
             pltpu.VMEM((128, 128), BF16),
+            pltpu.VMEM((5 * 112 + 3 * 128, 1024), BF16),
             pltpu.SemaphoreType.DMA((16,)),
-            pltpu.SemaphoreType.DMA((COPIES,)),
-            pltpu.SemaphoreType.DMA((COPIES,)),
+            pltpu.SemaphoreType.DMA((SENT,)),
+            pltpu.SemaphoreType.DMA((GOT,)),
         ],
         compiler_params=pltpu.CompilerParams(
             collective_id=0, has_side_effects=True, vmem_limit_bytes=60 * 1024 * 1024

time: 103 us -> 96.5 us (0.937)
  Pallas kernels: 102 us -> 95.6 us
    pallas_call x1, Pallas kernels: 102 us -> 95.6 us  [layer(): pl.pallas_call(layer_kernel, out_shape=pltpu.VMEM((tokens, width), BF16),...]
where the time goes in v6:
time: 96.5 us; the launch traced here: 96.4 us
  Pallas kernels  95.6 us (99%)
    pallas_call x1, Pallas kernels, layer(): pl.pallas_call(layer_kernel, out_shape=pltpu.VMEM((tokens, width), BF16),...  95.6 us

profile of v6, /device:TPU:1, one launch (start us, length us, event | category | flops | bytes accessed | tf_op | source)
XLA Modules:
  0.0 96.4 jit_solution(14974176104897899275)
XLA Ops:
  0.0 95.6 %layer.1 = bf16[128,2048]{1,0:T(8,128)(2,1)S(1)} custom-call(bf16[128,2048]{1,0:T(8,128)(2,1)} %bitcast.13, bf16[128,512]{1,0:T(8,128)(2,1)} %bitcast.15, bf16[128,512]{1,0:T(8,128)(2,1)} %bitcast.16, bf16[2048,2048]{1,0:T(8,128)(2,1)} %w_hbm.1, bf16[128,2048]{1,0:T(8,128)(2,1)} %bitcast.14, bf16[1,2048,512]{2,1,0:T(8,128)(2,1)} %gate_hbm.1, ...), custom_call_target="tpu_custom_call" | custom-call | tf_op jit(solution)/shard_map/layer/pallas_call | solution.py:609
  95.6 0.8 copy.18

commit v7 on v6

--- a/solution.py
+++ b/solution.py
@@ -88,10 +88,10 @@
         pltpu.make_async_copy(like, like, self.send_sem.at[self.sent_at[sent]]).wait()
 
 
-SPANS = {"d": (256, 512, 768, 512), "r": (512, 768, 512, 256)}
+SPANS = {"d": (256, 768, 768, 256), "r": (512, 768, 512, 256)}
 ROUNDS = 4
-SENT = 5 + 4 * ROUNDS
-GOT = 21 + 2 * 8 * ROUNDS
+SENT = 6
+GOT = 11 + 2 * 8 * ROUNDS
 
 
 def iota(shape, dim):
@@ -118,47 +118,30 @@
     to_y = {(s, o): at(z, x, y + s, c if o == 0 else 1 - c) for s in range(4) for o in (0, 1)}
     del to_y[0, 0]
     ring = {"z": (to_z[1], to_z[3]), "x": (to_x[1], to_x[3])}
+    loads = {}
+
+    def load(*items):
+        for name, src, dst in items:
+            loads[name] = pltpu.make_async_copy(src, dst, local_sem.at[len(loads)])
+            loads[name].start()
+
+    load(
+        ("v", v_hbm, v_raw), ("k", k_hbm, k_raw), ("table", table_hbm, table_ref),
+        ("kg", kg_hbm, kg_ref),
+    )
     barrier = pltpu.get_barrier_semaphore()
     peers = [*to_z.values(), *to_x.values(), *to_y.values()]
     for peer in peers:
         pl.semaphore_signal(barrier, inc=1, device_id=peer, device_id_type=MESH)
-    loads = {}
-    for i, (name, src, dst) in enumerate(
-        [
-            ("table", table_hbm, table_ref), ("k", k_hbm, k_raw), ("kg", kg_hbm, kg_ref),
-            ("v", v_hbm, v_raw), ("ids", ids_hbm, ids_ref), ("gw", gw_hbm, gw_ref),
-            ("fs", fs_hbm, fs_ref), ("qg", qg_hbm, qg_ref), ("q", q_hbm, q_raw),
-            ("postg", postg_hbm, postg_ref), ("preg", preg_hbm, preg_ref), ("res", res_hbm, res),
-            ("w", w_hbm, w), ("gate", gate_hbm.at[0], gate), ("up", up_hbm.at[0], up),
-            ("down", down_hbm.at[0], down),
-        ]
-    ):
-        loads[name] = pltpu.make_async_copy(src, dst, local_sem.at[i])
-        loads[name].start()
+    load(
+        ("ids", ids_hbm, ids_ref), ("gw", gw_hbm, gw_ref),
+        ("fs", fs_hbm, fs_ref), ("qg", qg_hbm, qg_ref), ("q", q_hbm, q_raw),
+        ("postg", postg_hbm, postg_ref), ("preg", preg_hbm, preg_ref), ("res", res_hbm, res),
+        ("w", w_hbm, w), ("gate", gate_hbm.at[0], gate), ("up", up_hbm.at[0], up),
+        ("down", down_hbm.at[0], down),
+    )
     ex = Exchange(send_sem, recv_sem)
 
-    lane = iota((GRID_W, HEAD_DIM), 1)
-
-    def table(which):
-        halves = []
-        for part in range(2):
-            row = table_ref[which, pl.ds(2 * (z * RING + x) + part, 1), :]
-            halves.append(jnp.where(lane < 64, row, table_ref[which, 32 : 32 + GRID_W, :]))
-        return jnp.concatenate(halves, axis=0)
-
-    loads["table"].wait()
-    cos, sin = table(0), table(1)
-    for name in ("ids", "gw", "fs"):
-        loads[name].wait()
-    meta[0, 0:2, :] = ids_ref[...].astype(F32)
-    meta[0, 2:3, :] = gw_ref[...]
-    meta[0, 3:4, :] = fs_ref[...]
-    meta[0, 4:8, :] = jnp.zeros((4, 128), F32)
-    loads["k"].wait()
-    loads["kg"].wait()
-    for h in range(KV_HEADS):
-        raw = k_raw[:, h * 128 : (h + 1) * 128].astype(F32)
-        kv[h // 2, 0, 0, :, (h % 2) * 128 : (h % 2 + 1) * 128] = turn(raw, kg_ref[...], cos, sin)
     loads["v"].wait()
     for half in range(2):
         kv[half, 0, 0, :, 256:512] = v_raw[:, half * 256 : (half + 1) * 256]
@@ -170,7 +153,7 @@
     second = ("z", "x")
     low, high = pl.ds(0, 64), pl.ds(64, 64)
 
-    def both(p, kind, r=0):
+    def both(p, kind, r=0, lanes=slice(None)):
         if kind == "own":
             peer = ring[first[p]]
             pairs = (kv.at[p, 0, 0], kv.at[p, 0, 3]), (kv.at[p, 0, 0], kv.at[p, 0, 1])
@@ -190,16 +173,41 @@
                 (kv.at[p, 1, r, high], kv.at[p, 2, r, high]),
             )
         for (src, dst), to in zip(pairs, peer):
-            ex.start(kind, (kind, p, r), src, dst, to)
-
-    def got(p, kind, r=0):
-        whole = kind in ("own", "far")
-        ex.arrived((kind, p, r), kv.at[p, 0, pl.ds(0, 2 if whole else 1)])
-
-    for p in range(2):
-        both(p, "own")
-    for p in range(2):
-        both(p, "far", 0)
+            ex.start("kv", (kind, r), src.at[:, lanes], dst.at[:, lanes], to)
+
+    def got(kind, r=0):
+        ex.arrived((kind, r), kv.at[0, 0, pl.ds(0, 4 if kind in ("own", "far") else 2)])
+
+    def own(lanes):
+        for kind in ("own", "far"):
+            for p in range(2):
+                both(p, kind, 0, lanes)
+
+    own(pl.ds(256, 256))
+    phase("kturn")
+    lane = iota((GRID_W, HEAD_DIM), 1)
+
+    def table(which):
+        halves = []
+        for part in range(2):
+            row = table_ref[which, pl.ds(2 * (z * RING + x) + part, 1), :]
+            halves.append(jnp.where(lane < 64, row, table_ref[which, 32 : 32 + GRID_W, :]))
+        return jnp.concatenate(halves, axis=0)
+
+    loads["table"].wait()
+    cos, sin = table(0), table(1)
+    for name in ("ids", "gw", "fs"):
+        loads[name].wait()
+    meta[0, 0:2, :] = ids_ref[...].astype(F32)
+    meta[0, 2:3, :] = gw_ref[...]
+    meta[0, 3:4, :] = fs_ref[...]
+    meta[0, 4:8, :] = jnp.zeros((4, 128), F32)
+    loads["k"].wait()
+    loads["kg"].wait()
+    for h in range(KV_HEADS):
+        raw = k_raw[:, h * 128 : (h + 1) * 128].astype(F32)
+        kv[h // 2, 0, 0, :, (h % 2) * 128 : (h % 2 + 1) * 128] = turn(raw, kg_ref[...], cos, sin)
+    own(pl.ds(0, 256))
     for r in (1, 2, 3):
         ex.start("meta", "meta", meta.at[0], meta.at[4 - r], to_z[r])
 
@@ -208,11 +216,11 @@
     loads["qg"].wait()
     for h in range(HEADS):
         raw = q_raw[:, h * 128 : (h + 1) * 128].astype(F32)
-        qt[h // 4, (h % 4) * 128 : (h % 4 + 1) * 128, :] = turn(raw, qg_ref[...], cos, sin)
+        qt[h // 4, :, (h % 4) * 128 : (h % 4 + 1) * 128] = turn(raw, qg_ref[...], cos, sin).T
 
     phase("own")
+    got("own")
     for p in range(2):
-        got(p, "own")
         both(p, "relay")
     for r in (3, 1):
         for p in range(2):
@@ -239,11 +247,11 @@
     home[...] = (iota((128, 128), 1).astype(F32) == stand(target)).astype(BF16)
 
     phase("relay")
+    got("relay")
     for p in range(2):
-        got(p, "relay")
         both(p, "far", 2)
+    got("far", 0)
     for p in range(2):
-        got(p, "far", 0)
         both(p, "last", 0)
 
     phase("tables2")
@@ -295,9 +303,7 @@
                 return jnp.concatenate([kv[p, a, b, :, cols] for a, b in blocks], axis=0)
 
             keys, values = part(0), part(256)
-            scores = lax.dot_general(
-                keys, qt[g], (((1,), (1,)), ((), ())), preferred_element_type=F32
-            )
+            scores = jnp.dot(keys, qt[g], preferred_element_type=F32)
             peak = jnp.max(scores, axis=0, keepdims=True)
             if not opening:
                 before = top[g]
@@ -323,9 +329,9 @@
     attend([(0, 0), (0, 1), (0, 2), (0, 3)], opening=True)
 
     def step_on(r, kind):
-        for p in range(2):
-            got(p, kind, r)
-            if kind == "far":
+        got(kind, r)
+        if kind == "far":
+            for p in range(2):
                 both(p, "last", r)
 
     phase("far3")
@@ -398,8 +404,7 @@
     def z_out(tag, i, src, dst):
         cols = span_of(tag, i)
         for r in (2, 1, 3):
-            name = (tag, "z", i)
-            ex.start(name, name, src.at[r, :, cols], dst.at[4 - r, :, cols], to_z[r])
+            ex.start((tag, "z"), (tag, "z", i), src.at[r, :, cols], dst.at[4 - r, :, cols], to_z[r])
 
     def z_in(tag, i):
         ex.arrived((tag, "z", i), like(96, SPANS[tag][i]))
@@ -410,7 +415,7 @@
 
         def x_out(w, r, ref, to_ref, cols):
             ex.start(
-                (tag, i), (tag, "x", r, i) if w == "a" else (tag, i),
+                tag, (tag, "x", r, i) if w == "a" else (tag, i),
                 ref.at[r, :, :, :, cols], to_ref.at[4 - r, :, :, :, cols], to_x[r],
             )
 
@@ -422,7 +427,7 @@
         def y_out(w, r, ref, to_ref, cols):
             for ry, rc in sides:
                 ex.start(
-                    (tag, i), (tag, "y", r, i) if w == "b" and r else (tag, i),
+                    tag, (tag, "y", r, i) if w == "b" and r else (tag, i),
                     ref.at[r, ry, rc, :, cols], to_ref.at[r, (4 - ry) % 4, rc, :, cols],
                     to_y[ry, rc],
                 )
@@ -455,9 +460,8 @@
         ex.arrived((tag, i), like(5 * 112 + 3 * 128, step))
 
     def settle_swaps(tag):
-        for i in range(ROUNDS):
-            ex.settle((tag, "z", i), like(96, SPANS[tag][i]))
-            ex.settle((tag, i), like(4 * 112 + 3 * 128, SPANS[tag][i]))
+        ex.settle((tag, "z"), like(96, width))
+        ex.settle(tag, like(4 * 112 + 3 * 128, width))
 
     def run(steps, count):
         for _ in range(count):
@@ -521,10 +525,7 @@
         lift(i, 0, 4)
 
     begin(0)
-    ex.settle("own", kv.at[0, 0])
-    ex.settle("relay", kv.at[0, 0, pl.ds(0, 2)])
-    ex.settle("far", kv.at[0])
-    ex.settle("last", kv.at[0, pl.ds(0, 2)])
+    ex.settle("kv", tally)
     ex.settle("meta", meta.at[pl.ds(0, 3)])
     begin(1)
     middle(0)
@@ -575,8 +576,8 @@
     end(0)
     begin(3)
     middle(2)
+    middle(3)
     end(1)
-    middle(3)
     end(2)
     end(3)
 
@@ -621,7 +622,7 @@
             pltpu.VMEM((1, tokens), F32),
             pltpu.VMEM((1, tokens), F32),
             pltpu.VMEM((2, 4, 4, 128, 512), BF16),
-            pltpu.VMEM((4, 512, 128), BF16),
+            pltpu.VMEM((4, 128, 512), BF16),
             rows,
             pltpu.VMEM((tokens, 512), BF16),
             pltpu.VMEM((tokens, 512), BF16),
@@ -646,7 +647,7 @@
             pltpu.VMEM((128, 512), BF16),
             pltpu.VMEM((128, 512), BF16),
             pltpu.VMEM((128, 128), BF16),
-            pltpu.VMEM((5 * 112 + 3 * 128, 1024), BF16),
+            pltpu.VMEM((960, width), BF16),
             pltpu.SemaphoreType.DMA((16,)),
             pltpu.SemaphoreType.DMA((SENT,)),
             pltpu.SemaphoreType.DMA((GOT,)),

time: 96.5 us -> 95.6 us (level)
  no operation moved by 1% of the time
where the time goes in v7:
time: 95.6 us; the launch traced here: 95.5 us
  Pallas kernels  94.7 us (99%)
    pallas_call x1, Pallas kernels, layer(): pl.pallas_call(layer_kernel, out_shape=pltpu.VMEM((tokens, width), BF16),...  94.7 us

profile of v7, /device:TPU:1, one launch (start us, length us, event | category | flops | bytes accessed | tf_op | source)
XLA Modules:
  0.0 95.5 jit_solution(10542079214008634990)
XLA Ops:
  0.0 94.7 %layer.1 = bf16[128,2048]{1,0:T(8,128)(2,1)S(1)} custom-call(bf16[128,2048]{1,0:T(8,128)(2,1)} %bitcast.13, bf16[128,512]{1,0:T(8,128)(2,1)} %bitcast.15, bf16[128,512]{1,0:T(8,128)(2,1)} %bitcast.16, bf16[2048,2048]{1,0:T(8,128)(2,1)} %w_hbm.1, bf16[128,2048]{1,0:T(8,128)(2,1)} %bitcast.14, bf16[1,2048,512]{2,1,0:T(8,128)(2,1)} %gate_hbm.1, ...), custom_call_target="tpu_custom_call" | custom-call | tf_op jit(solution)/shard_map/layer/pallas_call | solution.py:610
  94.7 0.8 copy.18

commit v8 on v7

--- a/solution.py
+++ b/solution.py
@@ -178,12 +178,8 @@
     def got(kind, r=0):
         ex.arrived((kind, r), kv.at[0, 0, pl.ds(0, 4 if kind in ("own", "far") else 2)])
 
-    def own(lanes):
-        for kind in ("own", "far"):
-            for p in range(2):
-                both(p, kind, 0, lanes)
-
-    own(pl.ds(256, 256))
+    for p in range(2):
+        both(p, "own", 0, pl.ds(256, 256))
     phase("kturn")
     lane = iota((GRID_W, HEAD_DIM), 1)
 
@@ -207,7 +203,10 @@
     for h in range(KV_HEADS):
         raw = k_raw[:, h * 128 : (h + 1) * 128].astype(F32)
         kv[h // 2, 0, 0, :, (h % 2) * 128 : (h % 2 + 1) * 128] = turn(raw, kg_ref[...], cos, sin)
-    own(pl.ds(0, 256))
+    for p in range(2):
+        both(p, "own", 0, pl.ds(0, 256))
+    for p in range(2):
+        both(p, "far", 0)
     for r in (1, 2, 3):
         ex.start("meta", "meta", meta.at[0], meta.at[4 - r], to_z[r])
 

time: 95.6 us -> 95.4 us (level)
  no operation moved by 1% of the time
where the time goes in v8:
time: 95.4 us; the launch traced here: 95.3 us
  Pallas kernels  94.5 us (99%)
    pallas_call x1, Pallas kernels, layer(): pl.pallas_call(layer_kernel, out_shape=pltpu.VMEM((tokens, width), BF16),...  94.5 us

profile of v8, /device:TPU:1, one launch (start us, length us, event | category | flops | bytes accessed | tf_op | source)
XLA Modules:
  0.0 95.3 jit_solution(10746426264855741096)
XLA Ops:
  0.0 94.5 %layer.1 = bf16[128,2048]{1,0:T(8,128)(2,1)S(1)} custom-call(bf16[128,2048]{1,0:T(8,128)(2,1)} %bitcast.13, bf16[128,512]{1,0:T(8,128)(2,1)} %bitcast.15, bf16[128,512]{1,0:T(8,128)(2,1)} %bitcast.16, bf16[2048,2048]{1,0:T(8,128)(2,1)} %w_hbm.1, bf16[128,2048]{1,0:T(8,128)(2,1)} %bitcast.14, bf16[1,2048,512]{2,1,0:T(8,128)(2,1)} %gate_hbm.1, ...), custom_call_target="tpu_custom_call" | custom-call | tf_op jit(solution)/shard_map/layer/pallas_call | solution.py:609
  94.6 0.8 copy.18
